TPU v7x, 32 devices: a whole 2x2x4 slice. The times are simulated.
32 devices in a mesh: sp: 8 (over z, y), dp: 4 (over x, core).
Axes of the slice: x: 2, y: 2, z: 4, core: 2. Of those that a mesh axis runs over, the one named last changes fastest.
Arguments:
- query: bfloat16 [4, 1536, 3072], P('dp', 'sp'), may hold values from -18 to 18
- latent: bfloat16 [4, 1536, 1024], P('dp', 'sp'), may hold values from -6 to 6
- rope_key: bfloat16 [4, 1536, 32], P('dp', 'sp'), may hold values from -5 to 5
- latent_norm_gain: float32 [1024], replicated, may hold values from 0.1 to 1.9
- key_up_matrix: bfloat16 [2048, 1024], P('dp'), may hold values from -0.1875 to 0.1875
- value_up_matrix: bfloat16 [2048, 1024], P('dp'), may hold values from -0.1875 to 0.1875
- out_grad: bfloat16 [4, 1536, 2048], P('dp', 'sp'), may hold values from -6 to 6
Outputs:
- query_grad: bfloat16 [4, 1536, 3072], P('dp', 'sp')
- latent_grad: float32 [4, 1536, 1024], P('dp', 'sp')
- rope_key_grad: float32 [4, 1536, 32], P('dp', 'sp')
- key_weight_grad: float32 [2048, 1024], P('dp')
- value_weight_grad: float32 [2048, 1024], P('dp')
- gain_grad: float32 [1024], replicated
All inputs are finite; a program needn't handle non-finite values.
Results may differ from a plain program's by a relative error of at most 0.011.
Values may be sent and summed in bfloat16 or wider, within the bound.
A program may use at most 256 MiB of HBM per device.

v0:
```python
import functools
import math

import jax
import jax.numpy as jnp
from jax import lax
from jax.experimental import pallas as pl
from jax.experimental.pallas import tpu as pltpu
from jax.sharding import PartitionSpec as P

ATTENTION_HEADS = 32
PLAIN_HEAD_WIDTH = 64
ROPE = 32
VALUE_HEAD_WIDTH = 64
SPAN = 64
WIDTH = PLAIN_HEAD_WIDTH + ROPE

eps = 1e-06
rope_base = 10000.0


def rotate(values, cosine, sine):
    half = values.shape[-1] // 2
    first = values[..., :half]
    second = values[..., half:]
    return jnp.concatenate(
        [first * cosine - second * sine, second * cosine + first * sine], axis=-1
    )


def angles(length, width):
    inverse = 1.0 / rope_base ** (jnp.arange(0, width, 2, dtype=jnp.float32) / width)
    turned = jnp.arange(length, dtype=jnp.float32)[:, None] * inverse[None, :]
    return (jnp.cos(turned), jnp.sin(turned))


NT = (((1,), (1,)), ((), ()))
NN = (((1,), (0,)), ((), ()))


def mm(a, b, dims=NN):
    return lax.dot_general(a, b, dims, preferred_element_type=jnp.float32)


def attention_kernel(
    heads, tile,
    arrived, keyvals, k_rope, cosine, sine,
    grads_out, dr_out,
    q_s, go_s, k_s, kt_s, v_s, s_s, dp_s, dk_s, dv_s, dq_s,
):
    f32 = jnp.float32
    bf16 = jnp.bfloat16
    length = k_rope.shape[0]
    blocks = length // tile
    scale = WIDTH ** (-0.5)
    steep = scale * math.log2(math.e)
    half = ROPE // 2
    pid = pl.program_id(0)

    for h in range(heads):
        @pl.when(pid == h)
        def _():
            raw = arrived[:, h * WIDTH : (h + 1) * WIDTH]
            turned = rotate(
                raw[:, PLAIN_HEAD_WIDTH:].astype(f32), cosine[:, :half], sine[:, :half]
            ).astype(bf16)
            q_s[...] = jnp.concatenate([raw[:, :PLAIN_HEAD_WIDTH], turned], axis=1)
            base = heads * WIDTH + h * VALUE_HEAD_WIDTH
            go_s[...] = arrived[:, base : base + VALUE_HEAD_WIDTH]
            both = jnp.concatenate(
                [keyvals[:, h * PLAIN_HEAD_WIDTH : (h + 1) * PLAIN_HEAD_WIDTH], k_rope[...]], axis=1
            )
            k_s[...] = both
            base = heads * PLAIN_HEAD_WIDTH + h * VALUE_HEAD_WIDTH
            v_s[...] = keyvals[:, base : base + VALUE_HEAD_WIDTH]

    for b in range(blocks):
        kt_s[b] = k_s[b * tile : (b + 1) * tile, :].astype(f32).T.astype(bf16)
    dk_s[...] = jnp.zeros_like(dk_s)
    dv_s[...] = jnp.zeros_like(dv_s)

    key_seg = lax.broadcasted_iota(jnp.int32, (tile, tile), 0) // SPAN
    query_seg = lax.broadcasted_iota(jnp.int32, (tile, tile), 1) // SPAN

    def fold(x, op):
        return op(x.reshape(tile // 8, 8, tile), axis=0)

    def query_block(qi, _):
        rows = pl.ds(pl.multiple_of(qi * tile, tile), tile)
        q = q_s[rows, :]
        go = go_s[rows, :]

        def score(kb, peak, diagonal=False):
            at = pl.ds(pl.multiple_of(kb * tile, tile), tile)
            s = mm(k_s[at, :], q, NT)
            if diagonal:
                s = jnp.where(key_seg <= query_seg, s, -1e30)
            s_s[at, :] = s
            dp_s[at, :] = mm(v_s[at, :], go, NT)
            return jnp.maximum(peak, fold(s, jnp.max))

        peak = lax.fori_loop(0, qi, score, jnp.full((8, tile), -1e30, f32))
        peak = score(qi, peak, diagonal=True)
        top = jnp.max(peak, axis=0, keepdims=True) * steep

        def weigh(kb, carry):
            total, mixed = carry
            at = pl.ds(pl.multiple_of(kb * tile, tile), tile)
            p = jnp.exp2(s_s[at, :] * steep - top)
            s_s[at, :] = p
            return total + fold(p, jnp.sum), mixed + fold(p * dp_s[at, :], jnp.sum)

        zero = jnp.zeros((8, tile), f32)
        total, mixed = lax.fori_loop(0, qi + 1, weigh, (zero, zero))
        inverse = 1.0 / jnp.sum(total, axis=0, keepdims=True)
        delta = jnp.sum(mixed, axis=0, keepdims=True) * inverse

        dq_s[...] = jnp.zeros_like(dq_s)

        def spread(kb, _):
            at = pl.ds(pl.multiple_of(kb * tile, tile), tile)
            probs = s_s[at, :] * inverse
            ds = (probs * (dp_s[at, :] - delta)).astype(bf16)
            dv_s[at, :] += mm(probs.astype(bf16), go)
            dk_s[at, :] += mm(ds, q)
            dq_s[...] += mm(kt_s[kb], ds)
            return 0

        lax.fori_loop(0, qi + 1, spread, 0)
        dq = dq_s[...].T * scale
        back = rotate(dq[:, PLAIN_HEAD_WIDTH:], cosine[rows, :half], -sine[rows, :half])
        done = jnp.concatenate([dq[:, :PLAIN_HEAD_WIDTH], back], axis=1).astype(bf16)
        for h in range(heads):
            @pl.when(pid == h)
            def _():
                grads_out[rows, h * WIDTH : (h + 1) * WIDTH] = done
        return 0

    lax.fori_loop(0, blocks, query_block, 0)

    dk = dk_s[...] * scale
    for h in range(heads):
        @pl.when(pid == h)
        def _():
            base = heads * WIDTH + h * PLAIN_HEAD_WIDTH
            grads_out[:, base : base + PLAIN_HEAD_WIDTH] = dk[:, :PLAIN_HEAD_WIDTH].astype(bf16)
            base = heads * (WIDTH + PLAIN_HEAD_WIDTH) + h * VALUE_HEAD_WIDTH
            grads_out[:, base : base + VALUE_HEAD_WIDTH] = dv_s[...].astype(bf16)
            if h == 0:
                dr_out[...] = dk[:, PLAIN_HEAD_WIDTH:]
            else:
                dr_out[...] += dk[:, PLAIN_HEAD_WIDTH:]


def attend_backward(arrived, keyvals, k_rope, cosine, sine, heads):
    length = arrived.shape[0]
    tile = 256
    f32 = jnp.float32
    bf16 = jnp.bfloat16

    def whole(a):
        return pl.BlockSpec(a.shape, lambda i: (0,) * len(a.shape))

    outs = (
        jax.ShapeDtypeStruct((length, heads * (WIDTH + PLAIN_HEAD_WIDTH + VALUE_HEAD_WIDTH)), bf16),
        jax.ShapeDtypeStruct((length, ROPE), f32),
    )
    ins = (arrived, keyvals, k_rope, cosine, sine)
    return pl.pallas_call(
        functools.partial(attention_kernel, heads, tile),
        grid=(heads,),
        out_shape=outs,
        in_specs=[whole(a) for a in ins],
        out_specs=tuple(whole(a) for a in outs),
        scratch_shapes=[
            pltpu.VMEM((length, WIDTH), bf16),
            pltpu.VMEM((length, VALUE_HEAD_WIDTH), bf16),
            pltpu.VMEM((length, WIDTH), bf16),
            pltpu.VMEM((length // tile, WIDTH, tile), bf16),
            pltpu.VMEM((length, VALUE_HEAD_WIDTH), bf16),
            pltpu.VMEM((length, tile), f32),
            pltpu.VMEM((length, tile), f32),
            pltpu.VMEM((length, WIDTH), f32),
            pltpu.VMEM((length, VALUE_HEAD_WIDTH), f32),
            pltpu.VMEM((WIDTH, tile), f32),
        ],
        compiler_params=pltpu.CompilerParams(
            dimension_semantics=("arbitrary",), vmem_limit_bytes=56 * 1024 * 1024
        ),
        cost_estimate=pl.CostEstimate(
            flops=heads * length * length * 420, bytes_accessed=8 * length * 1024,
            transcendentals=heads * length * length // 2,
        ),
    )(*ins)


def normalise(latent):
    lat = latent.astype(jnp.float32)
    inv_rms = lax.rsqrt(jnp.mean(lat * lat, axis=-1, keepdims=True) + eps)
    return lat * inv_rms, inv_rms


def local(query, latent, rope_key, latent_norm_gain, key_up_matrix, value_up_matrix, out_grad):
    f32 = jnp.float32
    bf16 = jnp.bfloat16
    sp = lax.axis_size("sp")
    dp = lax.axis_size("dp")
    tokens, channels = latent.shape[1:]
    heads = ATTENTION_HEADS // sp
    ratio = sp // dp
    to_user = [
        (s * dp + d, (d * ratio + s // dp) * dp + s % dp) for s in range(sp) for d in range(dp)
    ]
    to_holder = [(b, a) for a, b in to_user]

    rope_all = lax.all_gather(rope_key[0], "sp", axis=0, tiled=True)
    stacked = jnp.stack([key_up_matrix, value_up_matrix])
    whole = lax.all_gather(stacked, "dp", axis=1, tiled=True)
    packed = jnp.concatenate(
        [
            query[0].reshape(tokens, sp, heads * WIDTH),
            out_grad[0].reshape(tokens, sp, heads * VALUE_HEAD_WIDTH),
        ],
        axis=-1,
    ).transpose(1, 0, 2)
    packed, rope_all = lax.optimization_barrier((packed, rope_all))
    arrived = lax.all_to_all(packed, "sp", split_axis=0, concat_axis=0, tiled=True)
    arrived = arrived.reshape(sp * tokens, -1)

    normed, inv_rms = normalise(latent[0])
    nlat = (normed * latent_norm_gain).astype(bf16)
    key_cols = lax.dot_general(nlat, whole[0], NT, preferred_element_type=f32).astype(bf16)
    value_cols = lax.dot_general(nlat, whole[1], NT, preferred_element_type=f32).astype(bf16)
    keyvals = jnp.concatenate(
        [
            key_cols.reshape(tokens, sp, heads * PLAIN_HEAD_WIDTH),
            value_cols.reshape(tokens, sp, heads * VALUE_HEAD_WIDTH),
        ],
        axis=-1,
    ).transpose(1, 0, 2)
    keyvals = lax.all_to_all(keyvals, "sp", split_axis=0, concat_axis=0, tiled=True)
    keyvals = keyvals.reshape(sp * tokens, -1)

    nlat_late, whole = lax.optimization_barrier((nlat, whole))
    nlat_all = lax.all_gather(nlat_late, "sp", axis=0, tiled=True)

    length = sp * tokens
    cosine, sine = angles(length, ROPE)
    k_rope = rotate(rope_all.astype(f32), cosine, sine).astype(bf16)

    grads, dr = attend_backward(arrived, keyvals, k_rope, cosine, sine, heads)
    split = heads * WIDTH
    own_keys = heads * PLAIN_HEAD_WIDTH

    returned = lax.all_to_all(
        grads.reshape(sp, tokens, -1), "sp", split_axis=0, concat_axis=0, tiled=True
    )
    weight_part = lax.dot_general(
        grads[:, split:], nlat_all, (((0,), (0,)), ((), ())), preferred_element_type=f32
    ).astype(bf16)
    weight_part = weight_part.reshape(2, -1, channels)
    weight_sum = lax.psum_scatter(weight_part, "dp", scatter_dimension=1, tiled=True)
    weight_sum = lax.ppermute(weight_sum, ("sp", "dp"), to_holder)
    weight_grads = lax.all_gather(weight_sum, "sp", axis=1, tiled=True).astype(f32)

    rope_parts = rotate(dr, cosine, -sine).reshape(sp, -1, tokens)
    rope_parts = lax.all_to_all(rope_parts, "sp", split_axis=0, concat_axis=0, tiled=True)
    rope_grad = jnp.sum(rope_parts, axis=0).reshape(tokens, ROPE)

    query_grad = returned[:, :, :split].transpose(1, 0, 2).reshape(tokens, -1)
    dk = returned[:, :, split : split + own_keys].transpose(1, 0, 2).reshape(tokens, -1)
    dv = returned[:, :, split + own_keys :].transpose(1, 0, 2).reshape(tokens, -1)
    d_nlat = lax.dot_general(dk, whole[0], NN, preferred_element_type=f32)
    d_nlat = d_nlat + lax.dot_general(dv, whole[1], NN, preferred_element_type=f32)
    gain_grad = lax.psum(jnp.sum(d_nlat * normed, axis=0), ("sp", "dp"))
    scaled = d_nlat * latent_norm_gain
    latent_grad = inv_rms * (scaled - normed * jnp.mean(scaled * normed, axis=-1, keepdims=True))
    return (
        query_grad[None],
        latent_grad[None],
        rope_grad[None],
        weight_grads[0],
        weight_grads[1],
        gain_grad,
    )


def solution(mesh):
    in_specs = (
        P("dp", "sp", None),
        P("dp", "sp", None),
        P("dp", "sp", None),
        P(),
        P("dp", None),
        P("dp", None),
        P("dp", "sp", None),
    )
    out_specs = (
        P("dp", "sp", None),
        P("dp", "sp", None),
        P("dp", "sp", None),
        P("dp", None),
        P("dp", None),
        P(),
    )
    return jax.shard_map(local, mesh=mesh, in_specs=in_specs, out_specs=out_specs, check_vma=False)
```

profile of v0, /device:TPU:3, one launch (start us, length us, event | category | flops | bytes accessed | tf_op | source)
XLA Modules:
  0.0 392.9 jit_solution(5427362936669306915)
XLA Ops:
  7.2 3.1 pad_maximum_fusion
  12.1 25.4 %all-gather = bf16[1,1536,32]{2,1,0:T(8,128)(2,1)S(1)} all-gather(bf16[1,192,32]{2,1,0:T(8,128)(2,1)S(1)} %copy.69), channel_id=2, replica_groups=mesh['sp'=8,'dp'=4] {'sp'}, dimensions={1}, use_global_device_ids=true | all-gather | bytes 110592 | tf_op jit(solution)/shard_map/all_gather | solution.py:216
  39.0 5.2 %all-to-all-start = ((bf16[8,192,640]{2,1,0:T(8,128)(2,1)}), bf16[8,192,640]{2,1,0:T(8,128)(2,1)S(1)}, u32[]{:S(2)}, u32[]{:S(2)}) async-start(bf16[8,192,640]{2,1,0:T(8,128)(2,1)} %maximum_bitcast_fusion), calls=%async_computation | async-start | bytes 3932160 | tf_op jit(solution)/shard_map/all_to_all | solution.py:227
  45.3 24.0 %all-gather.5.cloned.1.call-done = bf16[2,2048,1024]{2,1,0:T(8,128)(2,1)} async-done(((bf16[2,512,1024]{2,1,0:T(8,128)(2,1)}), bf16[2,2048,1024]{2,1,0:T(8,128)(2,1)}) %all-gather.5.cloned.1.call-update) | async-done | bytes 8388624 | tf_op jit(solution)/shard_map/all_gather | solution.py:218
  69.3 3.7 fusion.9
  73.0 3.7 fusion.8
  78.3 10.3 %all-to-all-done = bf16[8,192,640]{2,1,0:T(8,128)(2,1)S(1)} async-done(((bf16[8,192,640]{2,1,0:T(8,128)(2,1)}), bf16[8,192,640]{2,1,0:T(8,128)(2,1)S(1)}, u32[]{:S(2)}, u32[]{:S(2)}) %all-to-all-start) | async-done | bytes 1966112 | tf_op jit(solution)/shard_map/all_to_all | solution.py:227
  88.5 10.9 %all-to-all-start.1 = ((bf16[8,192,512]{2,1,0:T(8,128)(2,1)}), bf16[8,192,512]{2,1,0:T(8,128)(2,1)}, u32[]{:S(2)}, u32[]{:S(2)}) async-start(bf16[8,192,512]{2,1,0:T(8,128)(2,1)} %maximum_bitcast_fusion.1), calls=%async_computation.1 | async-start | bytes 3145728 | tf_op jit(solution)/shard_map/all_to_all | solution.py:241
  99.5 3.3 multiply_subtract_fusion.1
  104.1 3.7 fusion.33
  107.8 36.5 %all-to-all-done.1 = bf16[8,192,512]{2,1,0:T(8,128)(2,1)} async-done(((bf16[8,192,512]{2,1,0:T(8,128)(2,1)}), bf16[8,192,512]{2,1,0:T(8,128)(2,1)}, u32[]{:S(2)}, u32[]{:S(2)}) %all-to-all-start.1) | async-done | bytes 1572896 | tf_op jit(solution)/shard_map/all_to_all | solution.py:241
  144.4 74.7 %shard_map.118 = (bf16[1536,896]{1,0:T(8,128)(2,1)}, f32[1536,32]{1,0:T(8,128)}) custom-call(bf16[1536,640]{1,0:T(8,128)(2,1)} %bitcast.97, bf16[1536,512]{1,0:T(8,128)(2,1)} %bitcast.10.keyvals, bf16[1536,32]{1,0:T(8,128)(2,1)} %copy.75.k_rope, f32[1536,16]{1,0:T(8,128)} %get-tuple-element.59.cosine, f32[1536,16]{1,0:T(8,128)} %get-tuple-element.58.sine), custom_call_target="tpu_custom_call" | custom-call | flops 3963617280 | bytes 12582912 | tf_op jit(solution)/shard_map/pallas_call | solution.py:169
  219.0 4.8 %multiply_subtract_fusion = (f32[1536,16]{1,0:T(8,128)S(1)}, f32[1536,16]{1,0:T(8,128)S(1)}) fusion(f32[1536,32]{1,0:T(8,128)} %get-tuple-element.16, f32[16]{0:T(128)S(1)} %negate_power_fusion), kind=kLoop, calls=%fused_computation.45 | loop fusion | flops 196608 | bytes 393280 | tf_op jit(solution)/shard_map/sub | solution.py:27
  224.3 25.6 %all_to_all.20 = f32[8,32,192]{2,1,0:T(8,128)S(1)} all-to-all(f32[8,32,192]{2,1,0:T(8,128)S(1)} %reshape.94), channel_id=1, replica_groups=mesh['sp'=8,'dp'=4] {'sp'}, dimensions={0} | all-to-all | bytes 393216 | tf_op jit(solution)/shard_map/all_to_all | solution.py:267
  249.9 3.6 all-to-all-start.2
  253.7 5.1 %fusion.12 = bf16[512,1024]{1,0:T(8,128)(2,1)} fusion(bf16[1536,1024]{1,0:T(8,128)(2,1)} %all-gather.7.cloned.1.call-done, bf16[1536,896]{1,0:T(8,128)(2,1)} %get-tuple-element.14), kind=kOutput, calls=%fused_computation.19 | convolution fusion | flops 1611137024 | bytes 5767168 | tf_op jit(solution)/shard_map/dot_general | solution.py:258
  258.9 28.9 %reduce-scatter.2.cloned.1.call-done = bf16[2,64,1024]{2,1,0:T(8,128)(2,1)} async-done(((bf16[2,256,1024]{2,1,0:T(8,128)(2,1)}), bf16[2,64,1024]{2,1,0:T(8,128)(2,1)}) %reduce-scatter.2.cloned.1.call-update) | async-done | bytes 262160 | tf_op jit(solution)/shard_map/reduce_scatter | solution.py:262
  287.8 5.7 %collective-permute-start = (bf16[2,64,1024]{2,1,0:T(8,128)(2,1)}, bf16[2,64,1024]{2,1,0:T(8,128)(2,1)}, u32[]{:S(2)}, u32[]{:S(2)}) collective-permute-start(bf16[2,64,1024]{2,1,0:T(8,128)(2,1)} %reduce-scatter.2.cloned.1.call-done), channel_id=1, source_target_pairs={{0,0},{8,1},{16,2},{24,3},{1,4},{9,5},{17,6},{25,7},{2,8},{10,9},{... | collective-permute-start | bytes 786440 | tf_op jit(solution)/shard_map/ppermute | solution.py:263
  293.4 15.0 %collective-permute-done = bf16[2,64,1024]{2,1,0:T(8,128)(2,1)} collective-permute-done((bf16[2,64,1024]{2,1,0:T(8,128)(2,1)}, bf16[2,64,1024]{2,1,0:T(8,128)(2,1)}, u32[]{:S(2)}, u32[]{:S(2)}) %collective-permute-start) | collective-permute-done | bytes 262176 | tf_op jit(solution)/shard_map/ppermute | solution.py:263
  309.2 7.9 %all-to-all-done.2 = bf16[8,192,896]{2,1,0:T(8,128)(2,1)S(1)} async-done(((bf16[8,192,896]{2,1,0:T(8,128)(2,1)}), bf16[8,192,896]{2,1,0:T(8,128)(2,1)S(1)}, u32[]{:S(2)}, u32[]{:S(2)}) %all-to-all-start.2) | async-done | bytes 2752544 | tf_op jit(solution)/shard_map/all_to_all | solution.py:255
  319.0 3.0 broadcast_in_dim_reshape.6
  322.4 3.2 fusion.2
  325.6 3.4 fusion.29
  328.9 52.0 %psum.7 = f32[1024]{0:T(1024)} all-reduce(f32[1024]{0:T(1024)S(1)} %get-tuple-element.48), channel_id=1, replica_groups=mesh['sp'=8,'dp'=4] {'sp','dp'}, use_global_device_ids=true, to_apply=%region_5.0 | all-reduce | flops 1024 | bytes 8192 | tf_op jit(solution)/shard_map/psum | solution.py:275
  (53 shorter events, 16.3 us)
Async XLA Ops:
  7.2 62.1 %all-gather.5.cloned.1.call-start = ((), (), s32[]{:S(2)}) async-start(), calls=%async_computation.5 | async-start | bytes 10485760 | tf_op jit(solution)/shard_map/all_gather | solution.py:218
  7.2 3.2 copy-start.3
  10.3 1.3 copy-start.2
  10.7 1.3 copy-start.5
  39.0 5.2 %copy-start = (bf16[1,192,1024]{2,1,0:T(8,128)(2,1)S(1)}, bf16[1,192,1024]{2,1,0:T(8,128)(2,1)}, u32[]{:S(2)}) copy-start(bf16[1,192,1024]{2,1,0:T(8,128)(2,1)} %param.8) | copy-start | bytes 1179652
  39.0 5.4 %copy-start.4 = (f32[1024]{0:T(1024)S(1)}, f32[1024]{0:T(1024)}, u32[]{:S(2)}) copy-start(f32[1024]{0:T(1024)} %param.10) | copy-start | bytes 12292
  39.0 49.5 %all-to-all-start = ((bf16[8,192,640]{2,1,0:T(8,128)(2,1)}), bf16[8,192,640]{2,1,0:T(8,128)(2,1)S(1)}, u32[]{:S(2)}, u32[]{:S(2)}) async-start(bf16[8,192,640]{2,1,0:T(8,128)(2,1)} %maximum_bitcast_fusion), calls=%async_computation | async-start | bytes 3932160 | tf_op jit(solution)/shard_map/all_to_all | solution.py:227
  44.2 209.5 %all-gather.7.cloned.1.call-start = ((), (), s32[]{:S(2)}) async-start(), calls=%async_computation.6 | async-start | bytes 3538944 | tf_op jit(solution)/shard_map/all_gather | solution.py:245
  88.5 14.3 %copy-start.1 = (bf16[8,192,640]{2,1,0:T(8,128)(2,1)}, bf16[8,192,640]{2,1,0:T(8,128)(2,1)S(1)}, u32[]{:S(2)}) copy-start(bf16[8,192,640]{2,1,0:T(8,128)(2,1)S(1)} %all-to-all-done) | copy-start | bytes 5898244
  88.5 55.8 %all-to-all-start.1 = ((bf16[8,192,512]{2,1,0:T(8,128)(2,1)}), bf16[8,192,512]{2,1,0:T(8,128)(2,1)}, u32[]{:S(2)}, u32[]{:S(2)}) async-start(bf16[8,192,512]{2,1,0:T(8,128)(2,1)} %maximum_bitcast_fusion.1), calls=%async_computation.1 | async-start | bytes 3145728 | tf_op jit(solution)/shard_map/all_to_all | solution.py:241
  249.9 67.2 %all-to-all-start.2 = ((bf16[8,192,896]{2,1,0:T(8,128)(2,1)}), bf16[8,192,896]{2,1,0:T(8,128)(2,1)S(1)}, u32[]{:S(2)}, u32[]{:S(2)}) async-start(bf16[8,192,896]{2,1,0:T(8,128)(2,1)} %bitcast.96), calls=%async_computation.2 | async-start | bytes 5505024 | tf_op jit(solution)/shard_map/all_to_all | solution.py:255
  253.6 34.2 %reduce-scatter.2.cloned.1.call-start = ((), (), s32[]{:S(2)}) async-start(), calls=%async_computation.7 | async-start | bytes 1310720 | tf_op jit(solution)/shard_map/reduce_scatter | solution.py:262
  258.8 123.2 %all-gather.9.cloned.1.call-start = ((), (), s32[]{:S(2)}) async-start(), calls=%async_computation.8 | async-start | bytes 2359296 | tf_op jit(solution)/shard_map/all_gather | solution.py:264
  287.8 20.7 %collective-permute-start = (bf16[2,64,1024]{2,1,0:T(8,128)(2,1)}, bf16[2,64,1024]{2,1,0:T(8,128)(2,1)}, u32[]{:S(2)}, u32[]{:S(2)}) collective-permute-start(bf16[2,64,1024]{2,1,0:T(8,128)(2,1)} %reduce-scatter.2.cloned.1.call-done), channel_id=1, source_target_pairs={{0,0},{8,1},{16,2},{24,3},{1,4},{9,5},{17,6},{25,7},{2,8},{10,9},{... | collective-permute-start | bytes 786440 | tf_op jit(solution)/shard_map/ppermute | solution.py:263
Sparse Core Ops, SparseCore 0:
  10.5 58.7 all-gather.4
  71.5 89.3 all-gather.6
  258.9 28.7 reduce-scatter.1
  308.6 65.7 all-gather.8
where the time goes:
time: 395 us; the launch traced here: 393 us
  waiting for transfers between devices  123 us (31%)
  blocking collectives  103 us (26%)
  Pallas kernels  74.7 us (19%)
  starting transfers between devices  25.6 us (6%)
  other arithmetic  22.4 us (6%)
  matrix products  19.1 us (5%)
  between operations  14 us (4%)
  local copies, waits for them, and re-layouts  11.6 us (3%)
    pallas_call x1, Pallas kernels, attend_backward(): pl.pallas_call(functools.partial(attention_kernel, heads, tile), grid=(he...  74.7 us
    psum x1, blocking collectives, local(): gain_grad = lax.psum(jnp.sum(d_nlat * normed, axis=0), ('sp', 'dp'))  52 us
    all_to_all x1, waiting for transfers between devices, local(): lax.all_to_all(keyvals, 'sp', split_axis=0, concat_axis=0, tiled=True)  36.5 us
    reduce_scatter x1, waiting for transfers between devices, local(): lax.psum_scatter(weight_part, 'dp', scatter_dimension=1, tiled=True)  28.9 us
    all_to_all x1, blocking collectives, local(): lax.all_to_all(rope_parts, 'sp', split_axis=0, concat_axis=0, tiled=True)  25.6 us
    all_gather x1, blocking collectives, local(): rope_all = lax.all_gather(rope_key[0], 'sp', axis=0, tiled=True)  25.4 us
    all_gather x1, waiting for transfers between devices, local(): whole = lax.all_gather(stacked, 'dp', axis=1, tiled=True)  24 us
    ppermute x1, waiting for transfers between devices, local(): weight_sum = lax.ppermute(weight_sum, ('sp', 'dp'), to_holder)  15 us
  transfers between devices with their start and end apart: 8, of which 6 were waited for; matrix products, arithmetic and copies ran while one was open for 11% of the time, Pallas kernels for 19%

commit v1 on v0

v1 whole, which is shorter than its diff:
```python
import functools, math
import numpy as np
import jax, jax.numpy as jnp
from jax import lax
from jax.experimental import pallas as pl
from jax.experimental.pallas import tpu as pltpu
from jax.sharding import PartitionSpec as P
ATTENTION_HEADS = 32
PLAIN = 64
ROPE = 32
VALUE = 64
SPAN = 64
WIDTH = PLAIN + ROPE
LANES = 128
NT = (((1,), (1,)), ((), ()))
NN = (((1,), (0,)), ((), ()))
f32=jnp.float32; bf16=jnp.bfloat16
CH=64
MESH = pl.DeviceIdType.MESH
eps = 1e-06

NT = (((1,), (1,)), ((), ()))
TN = (((0,), (0,)), ((), ()))

def inner(n):
    return 2 ** ((n.bit_length() - 1) // 2)

def rcopy(src, dst, send, recv, dev):
    return pltpu.make_async_remote_copy(src_ref=src, dst_ref=dst, send_sem=send, recv_sem=recv, device_id=dev, device_id_type=MESH)

class Gather:
    def __init__(self, own, at, na, nb, a, b, dev, send, recv):
        self.own, self.at, self.na, self.nb, self.a, self.b, self.dev, self.send, self.recv = own, at, na, nb, a, b, dev, send, recv
        self.me = a * nb + b
    def copy(self, src, slot, way):
        a, b = self.a, self.b
        to = [(a + 1, b), (a - 1, b), (a, b + 1), (a, b - 1)][way]
        return rcopy(src, self.at(slot), self.send.at[slot, way], self.recv.at[slot], self.dev(*to))
    def can(self, way):
        return [self.a < self.na - 1, self.a > 0, self.b < self.nb - 1, self.b > 0][way]
    def go(self, src, slot, ways):
        for w in ways:
            @pl.when(self.can(w))
            def _(): self.copy(src, slot, w).start()
    def wait(self, slot):
        self.copy(self.own, slot, 0).wait_recv()
    def begin(self):
        self.go(self.own, self.me, (0, 1, 2, 3))
    def line(self, k, got=None):
        for sign, way in ((-1, 0), (1, 1)):
            far = self.a + sign * k
            ok = far >= 0 if sign < 0 else far < self.na
            @pl.when(ok)
            def _():
                slot = far * self.nb + self.b
                self.wait(slot)
                self.go(self.at(slot), slot, (way, 2, 3))
                if got is not None: got(slot)
    def across(self, j, got=None):
        for sign, way in ((-1, 2), (1, 3)):
            far = self.b + sign * j
            ok = far >= 0 if sign < 0 else far < self.nb
            @pl.when(ok)
            def _():
                for aa in range(self.na):
                    slot = aa * self.nb + far
                    self.wait(slot)
                    self.go(self.at(slot), slot, (way,))
                    if got is not None: got(slot)
    def finish(self):
        for w in range(4):
            @pl.when(self.can(w))
            def _(): self.copy(self.own, self.me, w).wait_send()
        for k in range(1, self.na):
            for sign, way in ((-1, 0), (1, 1)):
                far = self.a + sign * k
                ok = far >= 0 if sign < 0 else far < self.na
                @pl.when(ok)
                def _():
                    slot = far * self.nb + self.b
                    for w in (way, 2, 3):
                        @pl.when(self.can(w))
                        def _(): self.copy(self.own, slot, w).wait_send()
        for j in range(1, self.nb - 1):
            for sign, way in ((-1, 2), (1, 3)):
                far = self.b + sign * j
                ok = far >= 0 if sign < 0 else far < self.nb
                @pl.when(ok)
                def _():
                    for aa in range(self.na):
                        slot = aa * self.nb + far
                        @pl.when(self.can(way))
                        def _(): self.copy(self.own, slot, way).wait_send()

def greet(n, m, s, d):
    b = pltpu.get_barrier_semaphore()
    for k in range(1, n):
        pl.semaphore_signal(b, inc=1, device_id=(lax.rem(s + k, n), d), device_id_type=MESH)
    for k in range(1, m):
        pl.semaphore_signal(b, inc=1, device_id=(s, lax.rem(d + k, m)), device_id_type=MESH)
    pl.semaphore_wait(b, n + m - 2)

def front_kernel(n, m, chunks, packed, nlat, kw, vw, arrived, nlat_all, k_all, v_all,
                 lsem, nsend, nrecv, wsend, wrecv, qsend, qrecv):
    s = lax.axis_index("sp"); d = lax.axis_index("dp")
    ny = inner(n)
    ratio = n // m
    rows = kw.shape[0] // ratio
    z, y = lax.div(s, ny), lax.rem(s, ny)
    x, c = lax.div(d, 2), lax.rem(d, 2)
    locals_ = [pltpu.make_async_copy(packed.at[s], arrived.at[s], lsem.at[0]),
               pltpu.make_async_copy(nlat, nlat_all.at[s], lsem.at[1]),
               pltpu.make_async_copy(kw, k_all.at[d], lsem.at[2]),
               pltpu.make_async_copy(vw, v_all.at[d], lsem.at[3])]
    for l in locals_: l.start()
    greet(n, m, s, d)
    g = Gather(nlat, lambda t: nlat_all.at[t], n // ny, ny, z, y, lambda a, b: (a * ny + b, d), nsend, nrecv)
    ws = []
    for j in range(ratio):
        part = pl.ds(lax.rem(s + j, ratio) * rows, rows)
        for i, (own, whole) in enumerate(((kw, k_all), (vw, v_all))):
            ws.append(Gather(own.at[part], lambda t, whole=whole, part=part: whole.at[t, part], m // 2, 2, x, c, lambda a, b: (s, a * 2 + b), wsend.at[2 * j + i], wrecv.at[2 * j + i]))
    g.begin()
    for w in ws: w.begin()
    cs = []
    for i, (lo, hi) in enumerate(chunks):
        for k in range(1, n):
            t = lax.rem(s + k, n)
            cp = rcopy(packed.at[t, :, lo:hi], arrived.at[s, :, lo:hi], qsend.at[i, k], qrecv.at[i, k], (t, d))
            cs.append(cp)
    late = len(cs)
    for cp in cs[:0]: cp.start()
    for k in range(1, n // ny): g.line(k)
    for cp in cs: cp.start()
    for w in ws:
        for k in range(1, m // 2): w.line(k)
    for j in range(1, ny): g.across(j)
    for w in ws: w.across(1)
    for cp in cs: cp.wait()
    g.finish()
    for w in ws: w.finish()
    for l in locals_: l.wait()

def front(packed, nlat, kw, vw, m, chunks, cid=11):
    n = packed.shape[0]
    ratio = n // m
    A = pl.BlockSpec(memory_space=pl.ANY)
    S = pltpu.SemaphoreType.DMA
    outs = (jax.ShapeDtypeStruct(packed.shape, bf16), jax.ShapeDtypeStruct((n, *nlat.shape), bf16),
            jax.ShapeDtypeStruct((m, *kw.shape), bf16), jax.ShapeDtypeStruct((m, *vw.shape), bf16))
    return pl.pallas_call(
        functools.partial(front_kernel, n, m, chunks), out_shape=outs, in_specs=[A] * 4, out_specs=(A,) * 4,
        scratch_shapes=[S((4,)), S((n, 4)), S((n,)), S((2 * ratio, m, 4)), S((2 * ratio, m)), S((len(chunks), n)), S((len(chunks), n))],
        compiler_params=pltpu.CompilerParams(collective_id=cid, has_side_effects=True, vmem_limit_bytes=60 * 1024 * 1024),
    )(packed, nlat, kw, vw)

def back_kernel(n, m, dq, dk, dv, dr, part, dq_in, dk_in, dv_in, dr_in, wg_all,
                pieces, summed, blocks, lsem, psend, precv, gsend, grecv, osend, orecv, rsend, rrecv):
    s = lax.axis_index("sp"); d = lax.axis_index("dp")
    ny = inner(n)
    ratio = n // m
    z, y = lax.div(s, ny), lax.rem(s, ny)
    tokens = dq.shape[1]
    greet(n, m, s, d)
    ps = []
    for k in range(1, m):
        t = lax.rem(d + k, m)
        ps.append(rcopy(part.at[t], pieces.at[k], psend.at[k], precv.at[k], (s, t)))
    for cp in ps: cp.start()
    own = pltpu.make_async_copy(part.at[d], pieces.at[0], lsem.at[0]); own.start()
    cs = []
    moves = ((dr, dr_in), (dk, dk_in), (dv, dv_in), (dq, dq_in))
    for i, (src, dst) in enumerate(moves):
        for k in range(1, n):
            t = lax.rem(s + k, n)
            cs.append(rcopy(src.at[t], dst.at[s], rsend.at[i, k], rrecv.at[i, k], (t, d)))
    ls = [pltpu.make_async_copy(src.at[s], dst.at[s], lsem.at[1 + i]) for i, (src, dst) in enumerate(moves)]
    for l in ls: l.start()
    own.wait()
    for cp in ps: cp.wait()
    total = pieces[0].astype(f32)
    for k in range(1, m): total = total + pieces[k].astype(f32)
    summed[...] = total.astype(bf16)
    g = Gather(summed, lambda t: blocks.at[t], n // ny, ny, z, y, lambda a, b: (a * ny + b, d), gsend, grecv)
    def pass_on(slot, src):
        owner, place = lax.div(slot, ratio), lax.rem(slot, ratio)
        @pl.when(owner != d)
        def _(): rcopy(src, wg_all.at[place, d], osend.at[slot], orecv.at[place, d], (s, owner)).start()
        @pl.when(owner == d)
        def _(): pltpu.make_async_copy(src, wg_all.at[place, d], osend.at[slot]).start()
    g.begin()
    pass_on(s, summed)
    for cp in cs: cp.start()
    for k in range(1, n // ny): g.line(k, lambda slot: pass_on(slot, blocks.at[slot]))
    for j in range(1, ny): g.across(j, lambda slot: pass_on(slot, blocks.at[slot]))
    for cp in cs: cp.wait()
    g.finish()
    for slot in range(n):
        owner, place = slot // ratio, slot % ratio
        @pl.when(owner != d)
        def _(): rcopy(summed, wg_all.at[place, d], osend.at[slot], orecv.at[place, d], (s, owner)).wait_send()
        @pl.when(owner == d)
        def _(): pltpu.make_async_copy(summed, wg_all.at[place, d], osend.at[slot]).wait()
    for p in range(m):
        @pl.when(p != d)
        def _():
            for place in range(ratio):
                rcopy(summed, wg_all.at[place, p], osend.at[0], orecv.at[place, p], (s, p)).wait_recv()
    for l in ls: l.wait()

def back(dq, dk, dv, dr, part, cid=12):
    n, m = dq.shape[0], part.shape[0]
    ratio = n // m
    A = pl.BlockSpec(memory_space=pl.ANY)
    S = pltpu.SemaphoreType.DMA
    outs = tuple(jax.ShapeDtypeStruct(a.shape, a.dtype) for a in (dq, dk, dv, dr)) + (jax.ShapeDtypeStruct((ratio, *part.shape), bf16),)
    shape = part.shape[1:]
    return pl.pallas_call(
        functools.partial(back_kernel, n, m), out_shape=outs, in_specs=[A] * 5, out_specs=(A,) * 5,
        scratch_shapes=[pltpu.VMEM((m, *shape), bf16), pltpu.VMEM(shape, bf16), pltpu.VMEM((n, *shape), bf16),
                        S((5,)), S((m,)), S((m,)), S((n, 4)), S((n,)), S((n,)), S((ratio, m)), S((4, n)), S((4, n))],
        compiler_params=pltpu.CompilerParams(collective_id=cid, has_side_effects=True, vmem_limit_bytes=60 * 1024 * 1024),
    )(dq, dk, dv, dr, part)

def mm(a, b, dims=NN):
    return lax.dot_general(a, b, dims, preferred_element_type=jnp.float32)

def weave(gens):
    gens = list(gens)
    while gens:
        for g in list(gens):
            try: next(g)
            except StopIteration: gens.remove(g)

def pair_backward(tile, heads, cos_t, sin_t, s_s, dp_s, p_s, ds_s):
    length = heads[0][3].shape[0]
    blocks = length // tile
    scale = WIDTH ** (-0.5)
    steep = scale * math.log2(math.e)
    half = ROPE // 2
    query_seg = lax.broadcasted_iota(jnp.int32, (8, tile), 1) // SPAN
    def at(b): return slice(b * tile, (b + 1) * tile)
    def fold(x, op):
        return op(x.reshape(x.shape[0] // 8, 8, tile), axis=0)
    peaks = {}
    items = [(h, qi) for h in range(len(heads)) for qi in range(blocks)]
    def first(n):
        h, qi = items[n]; odd, q_s, go_s, k_s, kt_s, v_s, _, _ = heads[h]
        q = q_s[at(qi), :]; go = go_s[at(qi), :]
        par = n % 2
        peak = None
        for kb in range(qi + 1):
            s = mm(k_s[at(kb), :], q, NT)
            if kb == qi:
                parts = []
                for j in range(tile // SPAN):
                    ok = jnp.broadcast_to((query_seg >= j)[None], (SPAN // 8, 8, tile)).reshape(SPAN, tile)
                    parts.append(jnp.where(ok, s[j * SPAN:(j + 1) * SPAN], -1e30))
                s = jnp.concatenate(parts, axis=0)
            s_s[par, at(kb), :] = s
            m = fold(s, jnp.max)
            peak = m if peak is None else jnp.maximum(peak, m)
            peaks[n] = peak
            yield
            dp_s[par, at(kb), :] = mm(v_s[at(kb), :], go, NT)
            yield
    def second(n):
        h, qi = items[n]; odd, q_s, go_s, k_s, kt_s, v_s, put_dq, _ = heads[h]
        par = n % 2
        top = jnp.max(peaks[n], axis=0, keepdims=True) * steep
        total = jnp.zeros((8, tile), f32); mixed = jnp.zeros((8, tile), f32)
        for c in range((qi + 1) * tile // CH):
            r = slice(c * CH, (c + 1) * CH)
            p = jnp.exp2(s_s[par, r, :] * steep - top)
            s_s[par, r, :] = p
            total = total + fold(p, jnp.sum)
            mixed = mixed + fold(p * dp_s[par, r, :], jnp.sum)
            if c % (tile // CH) == tile // CH - 1: yield
        inverse = 1.0 / jnp.sum(total, axis=0, keepdims=True)
        delta = jnp.sum(mixed, axis=0, keepdims=True) * inverse
        for c in range((qi + 1) * tile // CH):
            r = slice(c * CH, (c + 1) * CH)
            probs = s_s[par, r, :] * inverse
            p_s[h, r, at(qi)] = probs.astype(bf16)
            ds_s[h, r, at(qi)] = (probs * (dp_s[par, r, :] - delta)).astype(bf16)
            if c % (tile // CH) == tile // CH - 1: yield
        dq = mm(kt_s[:, : (qi + 1) * tile], ds_s[h, : (qi + 1) * tile, at(qi)]) * scale
        a = 0 if odd else PLAIN
        c_, s_ = cos_t[:, at(qi)], sin_t[:, at(qi)]
        x, y = dq[a : a + half], dq[a + half : a + ROPE]
        b = PLAIN if odd else 0
        put_dq(at(qi), dq[b : b + PLAIN].astype(bf16), jnp.concatenate([x * c_ + y * s_, y * c_ - x * s_], axis=0).astype(bf16))
        yield
    def last(h):
        odd, q_s, go_s, k_s, kt_s, v_s, _, put_kv = heads[h]
        for kb in range(blocks):
            dv = mm(p_s[h, at(kb), kb * tile :], go_s[kb * tile :, :])
            dk = mm(ds_s[h, at(kb), kb * tile :], q_s[kb * tile :, :])
            put_kv(at(kb), dk * scale, dv)
            yield
    weave([first(0)])
    for n, (h, qi) in enumerate(items):
        gens = [second(n)]
        if n + 1 < len(items): gens.append(first(n + 1))
        weave(gens)
        if qi == blocks - 1: weave([last(h)])

def tables(length):
    inverse = 1.0 / 10000.0 ** (np.arange(0, ROPE, 2, dtype=np.float32) / np.float32(ROPE))
    turned = np.arange(length, dtype=np.float32)[None, :] * inverse.astype(np.float32)[:, None]
    return np.cos(turned.astype(np.float64)).astype(np.float32), np.sin(turned.astype(np.float64)).astype(np.float32)

def attention_kernel(heads, tile, arrived, keyvals, rope2, move, cos_t, sin_t, dq_out, dk_out, dv_out, dr_out,
                     q_s, k_s, kt_s, v_s, s_s, dp_s, p_s, ds_s, dqt_s, tc_s, ts_s):
    length = k_s.shape[1]
    blocks = length // tile
    lane = lax.broadcasted_iota(jnp.int32, (tile, LANES), 1)
    low = lane < PLAIN
    def at(b): return slice(b * tile, (b + 1) * tile)
    for b in range(blocks):
        z = jnp.zeros((ROPE, tile), f32)
        c = cos_t[:, at(b)]; s = sin_t[:, at(b)]
        tc_s[at(b), :] = jnp.concatenate([c, c, z, c, c, z], axis=0).T
        ts_s[at(b), :] = jnp.concatenate([-s, s, z, -s, s, z], axis=0).T
    dr_out[...] = jnp.zeros_like(dr_out)
    def pair(p, _):
        for b in range(blocks):
            x = arrived[p, at(b), :2 * LANES]
            y = mm(x, move[...])
            tc = tc_s[at(b), :]; ts = ts_s[at(b), :]
            q_s[0, at(b), :] = (y[:, :128] * jnp.where(low, 1.0, tc) + y[:, 128:256] * ts).astype(bf16)
            q_s[1, at(b), :] = (y[:, 256:384] * jnp.where(low, tc, 1.0) + y[:, 384:] * ts).astype(bf16)
            kp = keyvals[p, at(b), :]; vp = keyvals[heads // 2 + p, at(b), :]
            rp = rope2[at(b), :]
            zero = jnp.zeros_like(vp)
            ke = jnp.where(low, kp, rp); ko = jnp.where(low, rp, kp)
            k_s[0, at(b), :] = ke; k_s[1, at(b), :] = ko
            kt_s[0, :, at(b)] = ke.astype(f32).T.astype(bf16)
            kt_s[1, :, at(b)] = ko.astype(f32).T.astype(bf16)
            v_s[0, at(b), :] = jnp.where(low, vp, zero); v_s[1, at(b), :] = jnp.where(low, zero, vp)
        def put_dq(h):
            def put(cols, plain, turned):
                dqt_s[p, h * WIDTH : h * WIDTH + PLAIN, cols] = plain
                dqt_s[p, h * WIDTH + PLAIN : (h + 1) * WIDTH, cols] = turned
            return put
        def put_kv(h):
            def put(rows, dk, dv):
                if h == 0:
                    dk_out[p, rows, :] = dk.astype(bf16)
                    dv_out[p, rows, :] = dv.astype(bf16)
                    dr_out[rows, :] += jnp.where(low, 0.0, dk)
                else:
                    dk_out[p, rows, :] = jnp.where(low, dk_out[p, rows, :], dk.astype(bf16))
                    dv_out[p, rows, :] = jnp.where(low, dv_out[p, rows, :], dv.astype(bf16))
                    dr_out[rows, :] += jnp.where(low, dk, 0.0)
            return put
        go = arrived.at[p, :, 2 * LANES : 3 * LANES]
        pair_backward(tile, [(h == 1, q_s.at[h], go, k_s.at[h], kt_s.at[h], v_s.at[h], put_dq(h), put_kv(h)) for h in range(2)],
                      cos_t, sin_t, s_s, dp_s, p_s, ds_s)
        return 0
    lax.fori_loop(0, heads // 2, pair, 0)
    for p in range(heads // 2):
        for b in range(blocks):
            dq_out[at(b), p * 2 * WIDTH : (p + 1) * 2 * WIDTH] = dqt_s[p, :, at(b)].astype(f32).T.astype(bf16)

def mover():
    m = np.zeros((256, 512), np.float32)
    for h in range(2):
        base = h * WIDTH
        A = h * 256; B = A + 128
        pl_at = 64 * h; r_at = 64 - 64 * h
        for i in range(PLAIN): m[base + i, A + pl_at + i] = 1
        for i in range(ROPE):
            m[base + PLAIN + i, A + r_at + i] = 1
            m[base + PLAIN + (i + ROPE // 2) % ROPE, B + r_at + i] = 1
    return m

def attend3(arrived, keyvals, rope2, heads, tile=256):
    length = rope2.shape[0]
    pairs = heads // 2
    cos_t, sin_t = tables(length)
    V = pl.BlockSpec(memory_space=pltpu.VMEM)
    outs = (jax.ShapeDtypeStruct((length, heads * WIDTH), bf16), jax.ShapeDtypeStruct((pairs, length, 128), bf16),
            jax.ShapeDtypeStruct((pairs, length, 128), bf16), jax.ShapeDtypeStruct((length, 128), f32))
    return pl.pallas_call(
        functools.partial(attention_kernel, heads, tile), out_shape=outs,
        in_specs=[V] * 6, out_specs=(V,) * 4,
        scratch_shapes=[
            pltpu.VMEM((2, length, 128), bf16), pltpu.VMEM((2, length, 128), bf16), pltpu.VMEM((2, 128, length), bf16), pltpu.VMEM((2, length, 128), bf16),
            pltpu.VMEM((2, length, tile), f32), pltpu.VMEM((2, length, tile), f32),
            pltpu.VMEM((2, length, length), bf16), pltpu.VMEM((2, length, length), bf16),
            pltpu.VMEM((pairs, 2 * WIDTH, length), bf16), pltpu.VMEM((length, 128), f32), pltpu.VMEM((length, 128), f32),
        ],
        compiler_params=pltpu.CompilerParams(vmem_limit_bytes=60 * 1024 * 1024),
        cost_estimate=pl.CostEstimate(flops=heads * length * length * 420, bytes_accessed=8 * length * 1024, transcendentals=heads * length * length // 2),
    )(arrived, keyvals, rope2, jnp.asarray(mover(), bf16), jnp.asarray(cos_t), jnp.asarray(sin_t))

def turn(values, cosine, sine):
    half = values.shape[-1] // 2
    first = values[..., :half]
    second = values[..., half:]
    return jnp.concatenate([first * cosine - second * sine, second * cosine + first * sine], axis=-1)


def local(query, latent, rope_key, gain, key_up, value_up, out_grad):
    sp = lax.axis_size("sp")
    dp = lax.axis_size("dp")
    tokens, channels = latent.shape[1:]
    length = sp * tokens
    heads = ATTENTION_HEADS // sp
    pairs = heads // 2
    ratio = sp // dp
    s = lax.axis_index("sp")
    cos_t, sin_t = tables(length)
    cosine = lax.dynamic_slice_in_dim(jnp.asarray(cos_t.T), s * tokens, tokens, 0)
    sine = lax.dynamic_slice_in_dim(jnp.asarray(sin_t.T), s * tokens, tokens, 0)

    packed = jnp.concatenate(
        [query[0].reshape(tokens, sp, heads * WIDTH), out_grad[0].reshape(tokens, sp, heads * VALUE)], axis=-1
    ).transpose(1, 0, 2)
    lat = latent[0].astype(f32)
    inv_rms = lax.rsqrt(jnp.mean(lat * lat, axis=-1, keepdims=True) + eps)
    normed = lat * inv_rms
    nlat = (normed * gain).astype(bf16)
    k_rope = turn(rope_key[0].astype(f32), cosine, sine).astype(bf16)
    gap = jnp.zeros((tokens, ROPE), bf16)
    sent = jnp.concatenate([nlat, k_rope, gap, k_rope, gap], axis=1)
    arrived, nlat_all, k_all, v_all = front(packed, sent, key_up, value_up, dp, ((0, heads * (WIDTH + VALUE)),))

    arrived = arrived.reshape(length, -1)
    nlat_all = nlat_all.reshape(length, -1)
    rope2 = nlat_all[:, channels:]
    nlat_all = nlat_all[:, :channels]
    k_all = k_all.reshape(-1, channels)
    v_all = v_all.reshape(-1, channels)
    own = heads * PLAIN
    k_own = lax.dynamic_slice_in_dim(k_all, s * own, own, 0)
    v_own = lax.dynamic_slice_in_dim(v_all, s * own, own, 0)
    keys = lax.dot_general(nlat_all, k_own, NT, preferred_element_type=f32).astype(bf16)
    vals = lax.dot_general(nlat_all, v_own, NT, preferred_element_type=f32).astype(bf16)
    kv = jnp.stack([a[:, j * LANES : (j + 1) * LANES] for a in (keys, vals) for j in range(pairs)])
    gap = jnp.zeros((length, PLAIN), bf16)
    arr = jnp.stack([jnp.concatenate([arrived[:, p * 2 * WIDTH : (p + 1) * 2 * WIDTH], gap, arrived[:, heads * WIDTH + p * LANES : heads * WIDTH + (p + 1) * LANES]], 1) for p in range(pairs)])
    dq, dk, dv, dr = attend3(arr, kv, rope2, heads)
    dkc = jnp.concatenate([dk[p] for p in range(pairs)], 1)
    dvc = jnp.concatenate([dv[p] for p in range(pairs)], 1)
    TN = (((0,), (0,)), ((), ()))
    part = jnp.concatenate([lax.dot_general(a, nlat_all, TN, preferred_element_type=f32).astype(bf16) for a in (dkc, dvc)])
    part = part.reshape(dp, -1, channels)
    drc = (dr[:, :ROPE] + dr[:, PLAIN : PLAIN + ROPE])
    dq, dk, dv, dr, wg = back(*(a.reshape(sp, tokens, -1) for a in (dq, dkc, dvc, drc)), part)
    query_grad = dq.transpose(1, 0, 2).reshape(tokens, -1)
    dk = dk.transpose(1, 0, 2).reshape(tokens, -1)
    dv = dv.transpose(1, 0, 2).reshape(tokens, -1)
    rope_grad = turn(jnp.sum(dr, axis=0), cosine, -sine)
    wg = wg.reshape(ratio, 2, own, channels).astype(f32)
    d_nlat = lax.dot_general(dk, k_all, NN, preferred_element_type=f32)
    d_nlat = d_nlat + lax.dot_general(dv, v_all, NN, preferred_element_type=f32)
    gain_grad = lax.psum(jnp.sum(d_nlat * normed, axis=0), ("sp", "dp"))
    scaled = d_nlat * gain
    latent_grad = inv_rms * (scaled - normed * jnp.mean(scaled * normed, axis=-1, keepdims=True))
    return (query_grad[None], latent_grad[None], rope_grad[None], wg[:, 0].reshape(-1, channels), wg[:, 1].reshape(-1, channels), gain_grad)


def solution(mesh):
    tok = P("dp", "sp", None)
    rows = P("dp", None)
    return jax.shard_map(local, mesh=mesh, in_specs=(tok, tok, tok, P(), rows, rows, tok), out_specs=(tok, tok, tok, rows, rows, P()), check_vma=False)
```

time: 395 us -> 331 us (0.84)
  Pallas kernels: 74.7 us -> 244 us
  waiting for transfers between devices: 123 us -> 0 us
  blocking collectives: 103 us -> 37.7 us
  starting transfers between devices: 25.6 us -> 0 us
  between operations: 14 us -> 0.94 us
  matrix products: 19.1 us -> 13.9 us
    pallas_call x1 -> x3, Pallas kernels: 74.7 us -> 244 us  [the longest x1 129 us: back(): pl.pallas_call(functools.partial(back_kernel, n, m), out_shape=outs, in_s...]
    all_to_all x3 -> x0, waiting for transfers between devices: 54.7 us -> none  [the longest x1 36.5 us: local(): lax.all_to_all(keyvals, 'sp', split_axis=0, concat_axis=0, tiled=True)]
    reduce_scatter x1 -> x0, waiting for transfers between devices: 28.9 us -> none  [local(): lax.psum_scatter(weight_part, 'dp', scatter_dimension=1, tiled=True)]
    all_to_all x1 -> x0, blocking collectives: 25.6 us -> none  [local(): lax.all_to_all(rope_parts, 'sp', split_axis=0, concat_axis=0, tiled=True)]
    all_gather x1 -> x0, blocking collectives: 25.4 us -> none  [local(): rope_all = lax.all_gather(rope_key[0], 'sp', axis=0, tiled=True)]
    all_gather x3 -> x0, waiting for transfers between devices: 24 us -> none  [the longest x1 24 us: local(): whole = lax.all_gather(stacked, 'dp', axis=1, tiled=True)]
    all_to_all x3 -> x0, starting transfers between devices: 19.7 us -> none  [the longest x1 10.9 us: local(): lax.all_to_all(keyvals, 'sp', split_axis=0, concat_axis=0, tiled=True)]
    ppermute x1 -> x0, waiting for transfers between devices: 15 us -> none  [local(): weight_sum = lax.ppermute(weight_sum, ('sp', 'dp'), to_holder)]
  transfers between devices with their start and end apart: 8 -> 0, of which waited for: 6 -> 0; matrix products, arithmetic and copies ran while one was open for 11% -> 0% of each run, Pallas kernels for 19% -> 0%
where the time goes in v1:
time: 331 us; the launch traced here: 328 us
  Pallas kernels  244 us (74%)
  blocking collectives  37.7 us (11%)
  other arithmetic  19.1 us (6%)
  matrix products  13.9 us (4%)
  local copies, waits for them, and re-layouts  12.9 us (4%)
    pallas_call x1, Pallas kernels, back(): pl.pallas_call(functools.partial(back_kernel, n, m), out_shape=outs, in_s...  129 us
    pallas_call x1, Pallas kernels, front(): pl.pallas_call(functools.partial(front_kernel, n, m, chunks), out_shape=o...  86.7 us
    psum x1, blocking collectives, local(): gain_grad = lax.psum(jnp.sum(d_nlat * normed, axis=0), ('sp', 'dp'))  37.7 us
    pallas_call x1, Pallas kernels, attend3(): pl.pallas_call(functools.partial(attention_kernel, heads, tile), out_shap...  28.3 us

profile of v1, /device:TPU:3, one launch (start us, length us, event | category | flops | bytes accessed | tf_op | source)
XLA Modules:
  0.0 328.3 jit_solution(3476934499967054102)
XLA Ops:
  0.7 1.2 fusion.22
  2.8 1.0 fusion.38
  3.9 1.2 fusion.16
  6.9 1.5 maximum_bitcast_fusion.packed
  8.3 86.7 %shard_map.163 = (bf16[8,192,640]{2,1,0:T(8,128)(2,1)}, bf16[8,192,1152]{2,1,0:T(8,128)(2,1)}, bf16[4,512,1024]{2,1,0:T(8,128)(2,1)}, bf16[4,512,1024]{2,1,0:T(8,128)(2,1)}) custom-call(bf16[8,192,640]{2,1,0:T(8,128)(2,1)} %maximum_bitcast_fusion.packed, bf16[192,1152]{1,0:T(8,128)(2,1)} %concatenate.42.nlat, bf16[512,1024]{1,0:T(8,128)(2,1)} %kw.1, ...), custom_call_target="tpu_custom_call" | custom-call | tf_op jit(solution)/shard_map/pallas_call | solution.py:151
  95.1 1.8 slice.99.rope2
  96.9 3.2 convolution_convert_fusion
  100.0 2.1 convolution_convert_fusion.1
  102.4 1.3 pad_maximum_fusion.1.keyvals
  105.4 1.8 pad_maximum_fusion.arrived
  107.2 28.3 %shard_map.164 = (bf16[1536,384]{1,0:T(8,128)(2,1)}, bf16[2,1536,128]{2,1,0:T(8,128)(2,1)}, bf16[2,1536,128]{2,1,0:T(8,128)(2,1)}, f32[1536,128]{1,0:T(8,128)}) custom-call(bf16[2,1536,384]{2,1,0:T(8,128)(2,1)} %pad_maximum_fusion.arrived, bf16[4,1536,128]{2,1,0:T(8,128)(2,1)} %pad_maximum_fusion.1.keyvals, bf16[1536,128]{1,0:T(8,128)(2,1)} %slice.99.rope2, ...), custom_call_target="tpu_custom_call" | custom-call | flops 3963617280 | bytes 12582912 | tf_op jit(solution)/shard_map/pallas_call | solution.py:385
  135.5 2.6 slice_add_fusion
  138.3 1.0 fusion.6
  141.9 1.0 pad_maximum_fusion.2
  143.9 128.8 %shard_map.165 = (bf16[8,192,384]{2,1,0:T(8,128)(2,1)}, bf16[8,192,256]{2,1,0:T(8,128)(2,1)}, bf16[8,192,256]{2,1,0:T(8,128)(2,1)}, f32[8,192,32]{2,1,0:T(8,128)}, bf16[2,4,128,1024]{3,2,1,0:T(8,128)(2,1)}) custom-call(bf16[8,192,384]{2,1,0:T(8,128)(2,1)} %bitcast.89, bf16[8,192,256]{2,1,0:T(8,128)(2,1)} %pad_maximum_fusion.3.dk, ...), custom_call_target="tpu_custom_call" | custom-call | tf_op jit(solution)/shard_map/pallas_call | solution.py:218
  272.7 2.0 copy.38
  274.8 1.4 broadcast_in_dim_reshape.3
  276.3 3.3 fusion.46
  279.6 1.1 fusion.33
  281.7 3.4 %fusion.21 = (f32[1024]{0:T(1024)S(1)}, f32[192]{0:T(256)S(1)}, f32[192,1024]{1,0:T(8,128)S(1)}) fusion(bf16[1,192,1024]{2,1,0:T(8,128)(2,1)S(1)} %copy-done, f32[192]{0:T(256)S(1)} %add_rsqrt_fusion, f32[1024]{0:T(1024)S(1)} %copy-done.10, f32[192,1024]{1,0:T(8,128)S(1)} %fusion.46, bf16[192,2048]{1,0:T(8,128)(2,1)S(1)} %bitcast.76, ...), kind=kOutput, calls=%fused_computation.29 | convolution fusion | flops 806878016 | bytes 6956544 | tf_op jit(solution)/shard_map/dot_general | solution.py:458
  285.0 37.7 %psum.7 = f32[1024]{0:T(1024)} all-reduce(f32[1024]{0:T(1024)S(1)} %get-tuple-element.44), channel_id=1, replica_groups=mesh['sp'=8,'dp'=4] {'sp','dp'}, use_global_device_ids=true, to_apply=%region_4.0 | all-reduce | flops 1024 | bytes 8192 | tf_op jit(solution)/shard_map/psum | solution.py:459
  322.8 1.1 fusion.20
  323.9 2.0 bitcast_convert_fusion
  325.9 2.3 fusion.43
  (49 shorter events, 9.5 us)
Async XLA Ops:
  0.6 5.4 %copy-start.3 = (bf16[1,192,2048]{2,1,0:T(8,128)(2,1)S(1)}, bf16[1,192,2048]{2,1,0:T(8,128)(2,1)}, u32[]{:S(2)}) copy-start(bf16[1,192,2048]{2,1,0:T(8,128)(2,1)} %param.18) | copy-start | bytes 2359300
  5.0 1.4 copy-start.2
  96.9 3.2 copy-start.9
  102.4 2.1 copy-start.1
  135.5 2.6 copy-start.8
  139.3 1.4 copy-start.7
  272.7 3.4 %copy-start.6 = (bf16[8,192,256]{2,1,0:T(8,128)(2,1)S(1)}, bf16[8,192,256]{2,1,0:T(8,128)(2,1)}, u32[]{:S(2)}) copy-start(bf16[8,192,256]{2,1,0:T(8,128)(2,1)} %get-tuple-element.28) | copy-start | bytes 2359300
  276.2 3.3 %copy-start.5 = (f32[8,192,32]{2,1,0:T(8,128)S(1)}, f32[8,192,32]{2,1,0:T(8,128)}, u32[]{:S(2)}) copy-start(f32[8,192,32]{2,1,0:T(8,128)} %get-tuple-element.30) | copy-start | bytes 589828
  279.5 2.0 copy-start.4
  279.6 2.1 copy-start
  279.6 2.1 copy-start.10

commit v2 on v1

v2 whole, which is shorter than its diff:
```python
import functools, math
import numpy as np
import jax, jax.numpy as jnp
from jax import lax
from jax.experimental import pallas as pl
from jax.experimental.pallas import tpu as pltpu
from jax.sharding import PartitionSpec as P
ATTENTION_HEADS = 32
PLAIN = 64
ROPE = 32
VALUE = 64
SPAN = 64
WIDTH = PLAIN + ROPE
LANES = 128
NT = (((1,), (1,)), ((), ()))
NN = (((1,), (0,)), ((), ()))
f32=jnp.float32; bf16=jnp.bfloat16
CH=64
MESH = pl.DeviceIdType.MESH
eps = 1e-06


def inner(n):
    return 2 ** ((n.bit_length() - 1) // 2)

def rcopy(src, dst, send, recv, dev):
    return pltpu.make_async_remote_copy(src_ref=src, dst_ref=dst, send_sem=send, recv_sem=recv, device_id=dev, device_id_type=MESH)

class Gather:
    def __init__(self, own, at, na, nb, a, b, dev, send, recv):
        self.own, self.at, self.na, self.nb, self.a, self.b, self.dev, self.send, self.recv = own, at, na, nb, a, b, dev, send, recv
        self.me = a * nb + b
    def copy(self, src, slot, way):
        a, b = self.a, self.b
        to = [(a + 1, b), (a - 1, b), (a, b + 1), (a, b - 1)][way]
        return rcopy(src, self.at(slot), self.send.at[slot, way], self.recv.at[slot], self.dev(*to))
    def can(self, way):
        return [self.a < self.na - 1, self.a > 0, self.b < self.nb - 1, self.b > 0][way]
    def go(self, src, slot, ways):
        for w in ways:
            @pl.when(self.can(w))
            def _(): self.copy(src, slot, w).start()
    def wait(self, slot):
        self.copy(self.own, slot, 0).wait_recv()
    def begin(self):
        self.go(self.own, self.me, (0, 1, 2, 3))
    def line(self, k, got=None):
        for sign, way in ((-1, 0), (1, 1)):
            far = self.a + sign * k
            ok = far >= 0 if sign < 0 else far < self.na
            @pl.when(ok)
            def _():
                slot = far * self.nb + self.b
                self.wait(slot)
                self.go(self.at(slot), slot, (way, 2, 3))
                if got is not None: got(slot)
    def across(self, j, got=None):
        for sign, way in ((-1, 2), (1, 3)):
            far = self.b + sign * j
            ok = far >= 0 if sign < 0 else far < self.nb
            @pl.when(ok)
            def _():
                for aa in range(self.na):
                    slot = aa * self.nb + far
                    self.wait(slot)
                    self.go(self.at(slot), slot, (way,))
                    if got is not None: got(slot)
    def finish(self):
        for w in range(4):
            @pl.when(self.can(w))
            def _(): self.copy(self.own, self.me, w).wait_send()
        for k in range(1, self.na):
            for sign, way in ((-1, 0), (1, 1)):
                far = self.a + sign * k
                ok = far >= 0 if sign < 0 else far < self.na
                @pl.when(ok)
                def _():
                    slot = far * self.nb + self.b
                    for w in (way, 2, 3):
                        @pl.when(self.can(w))
                        def _(): self.copy(self.own, slot, w).wait_send()
        for j in range(1, self.nb - 1):
            for sign, way in ((-1, 2), (1, 3)):
                far = self.b + sign * j
                ok = far >= 0 if sign < 0 else far < self.nb
                @pl.when(ok)
                def _():
                    for aa in range(self.na):
                        slot = aa * self.nb + far
                        @pl.when(self.can(way))
                        def _(): self.copy(self.own, slot, way).wait_send()


def mm(a, b, dims=NN):
    return lax.dot_general(a, b, dims, preferred_element_type=jnp.float32)

def weave(gens):
    gens = list(gens)
    while gens:
        for g in list(gens):
            try: next(g)
            except StopIteration: gens.remove(g)

def pair_backward(tile, heads, cos_t, sin_t, s_s, dp_s, p_s, ds_s, dk_s=None, dv_s=None):
    length = heads[0][3].shape[0]
    blocks = length // tile
    scale = WIDTH ** (-0.5)
    steep = scale * math.log2(math.e)
    depth, held = s_s.shape[0], p_s.shape[0]
    half = ROPE // 2
    query_seg = lax.broadcasted_iota(jnp.int32, (8, tile), 1) // SPAN
    def at(b): return slice(b * tile, (b + 1) * tile)
    half_rows = (blocks + 1) // 2
    def spot(kb, qi, count=1):
        if dk_s is not None:
            return kb, slice(0, tile)
        if kb < half_rows:
            row, col = kb, qi - kb
        else:
            row, col = blocks - 1 - kb, kb + 1 + qi - kb
        return row, slice(col * tile, (col + count) * tile)
    def fold(x, op):
        return op(x.reshape(x.shape[0] // 8, 8, tile), axis=0)
    peaks = {}
    items = [(h, qi) for h in range(len(heads)) for qi in range(blocks)]
    def first(n):
        h, qi = items[n]; odd, q_s, go_s, k_s, kt_s, v_s, _, _ = heads[h]
        q = q_s[at(qi), :]; go = go_s[at(qi), :]
        par = n % depth
        peak = None
        for kb in range(qi + 1):
            s = mm(k_s[at(kb), :], q, NT)
            if kb == qi:
                parts = []
                for j in range(tile // SPAN):
                    ok = jnp.broadcast_to((query_seg >= j)[None], (SPAN // 8, 8, tile)).reshape(SPAN, tile)
                    parts.append(jnp.where(ok, s[j * SPAN:(j + 1) * SPAN], -1e30))
                s = jnp.concatenate(parts, axis=0)
            s_s[par, at(kb), :] = s
            m = fold(s, jnp.max)
            peak = m if peak is None else jnp.maximum(peak, m)
            peaks[n] = peak
            yield
            dp_s[par, at(kb), :] = mm(v_s[at(kb), :], go, NT)
            yield
    def second(n):
        h, qi = items[n]; odd, q_s, go_s, k_s, kt_s, v_s, put_dq, _ = heads[h]
        par = n % depth
        top = jnp.max(peaks[n], axis=0, keepdims=True) * steep
        total = jnp.zeros((8, tile), f32); mixed = jnp.zeros((8, tile), f32)
        for c in range((qi + 1) * tile // CH):
            r = slice(c * CH, (c + 1) * CH)
            p = jnp.exp2(s_s[par, r, :] * steep - top)
            s_s[par, r, :] = p
            total = total + fold(p, jnp.sum)
            mixed = mixed + fold(p * dp_s[par, r, :], jnp.sum)
            if c % (tile // CH) == tile // CH - 1: yield
        inverse = 1.0 / jnp.sum(total, axis=0, keepdims=True)
        delta = jnp.sum(mixed, axis=0, keepdims=True) * inverse
        for c in range((qi + 1) * tile // CH):
            r = slice(c * CH, (c + 1) * CH)
            probs = s_s[par, r, :] * inverse
            kb, inside = divmod(c * CH, tile)
            row, cols = spot(kb, qi)
            p_s[h % held, row, inside : inside + CH, cols] = probs.astype(bf16)
            ds_s[h % held, row, inside : inside + CH, cols] = (probs * (dp_s[par, r, :] - delta)).astype(bf16)
            if c % (tile // CH) == tile // CH - 1: yield
        dq = None
        for kb in range(qi + 1):
            row, cols = spot(kb, qi)
            term = mm(kt_s[:, at(kb)], ds_s[h % held, row, :, cols])
            dq = term if dq is None else dq + term
        dq = dq * scale
        a = 0 if odd else PLAIN
        c_, s_ = cos_t[:, at(qi)], sin_t[:, at(qi)]
        x, y = dq[a : a + half], dq[a + half : a + ROPE]
        b = PLAIN if odd else 0
        if dk_s is not None:
            for kb in range(qi + 1):
                row, cols = spot(kb, qi)
                for acc, left, right in ((dv_s, p_s, go_s), (dk_s, ds_s, q_s)):
                    term = mm(left[h % held, row, :, cols], right[at(qi), :])
                    if kb == qi:
                        acc[at(kb), :] = term
                    else:
                        acc[at(kb), :] += term
        put_dq(at(qi), dq[b : b + PLAIN].astype(bf16), jnp.concatenate([x * c_ + y * s_, y * c_ - x * s_], axis=0).astype(bf16))
        yield
    def last(h):
        odd, q_s, go_s, k_s, kt_s, v_s, _, put_kv = heads[h]
        for kb in range(blocks):
            if dk_s is not None:
                put_kv(at(kb), dk_s[at(kb), :] * scale, dv_s[at(kb), :])
                continue
            row, cols = spot(kb, kb, blocks - kb)
            dv = mm(p_s[h % held, row, :, cols], go_s[kb * tile :, :])
            dk = mm(ds_s[h % held, row, :, cols], q_s[kb * tile :, :])
            put_kv(at(kb), dk * scale, dv)
            yield
    weave([first(0)])
    for n, (h, qi) in enumerate(items):
        gens = [second(n)]
        if n + 1 < len(items): gens.append(first(n + 1))
        weave(gens)
        if qi == blocks - 1: weave([last(h)])

def tables(length):
    inverse = 1.0 / 10000.0 ** (np.arange(0, ROPE, 2, dtype=np.float32) / np.float32(ROPE))
    turned = np.arange(length, dtype=np.float32)[None, :] * inverse.astype(np.float32)[:, None]
    return np.cos(turned.astype(np.float64)).astype(np.float32), np.sin(turned.astype(np.float64)).astype(np.float32)

PARTS = 2


def head_mover(pairs):
    m = np.zeros((min(pairs, 2), 2 * LANES, 4 * LANES), np.float32)
    for p in range(m.shape[0]):
        for h in range(2):
            base = p * 64 + h * WIDTH
            plain, turned = PLAIN * h, PLAIN - PLAIN * h
            for i in range(PLAIN):
                m[p, base + i, 2 * LANES * h + plain + i] = 1
            for i in range(ROPE):
                m[p, base + PLAIN + i, 2 * LANES * h + turned + i] = 1
                m[p, base + PLAIN + (i + ROPE // 2) % ROPE, 2 * LANES * h + LANES + turned + i] = 1
    return m


def rope_mover():
    m = np.zeros((ROPE, 2 * LANES), np.float32)
    for i in range(ROPE):
        for at in (0, PLAIN):
            m[i, at + i] = 1
            m[(i + ROPE // 2) % ROPE, LANES + at + i] = 1
    return m


class Plan:
    def __init__(self, n, m, tokens, channels):
        self.n, self.m, self.tokens, self.channels = n, m, tokens, channels
        self.length = n * tokens
        self.heads = ATTENTION_HEADS // n
        self.pairs = self.heads // 2
        self.ratio = n // m
        self.qw = self.heads * WIDTH
        self.own = self.heads * PLAIN
        self.tile = 256
        self.blocks = self.length // self.tile
        self.depth = 2 if self.length <= 2048 else 1
        self.hold = self.length <= 2048
        self.aligned = self.qw % LANES == 0
        qt = -(-self.qw // LANES)
        if self.pairs == 2 and self.qw == 3 * LANES:
            self.chunks = ((0, 3 * LANES), (3 * LANES, 5 * LANES))
            self.q_tiles = ((0, 1), (1, 3))
            self.go_tile = (2, 4)
            self.dq_cols = ((0, LANES), (LANES, 3 * LANES))
        else:
            self.chunks = ((0, (qt + self.pairs) * LANES),)
            self.q_tiles = tuple((p * 2 * WIDTH // LANES, p * 2 * WIDTH // LANES + 1) for p in range(self.pairs))
            self.go_tile = tuple(qt + p for p in range(self.pairs))
            self.dq_cols = ((0, 0),) * (self.pairs - 1) + ((0, self.qw),)
        self.wide = self.chunks[-1][1]
        self.direct = self.pairs == 2 and self.qw == 3 * LANES
        if self.direct:
            self.moves = (((0, 0, 2 * LANES, 0), (1, 0, LANES, 2 * LANES)), ((0, 2 * LANES, LANES, 3 * LANES), (1, LANES, LANES, 4 * LANES)))
        else:
            self.moves = (((2, 0, self.wide, 0),),)
            self.chunks = ((0, self.wide),)
        self.rows = 2 * self.own // m

    def pack(self, query, grad):
        if self.direct:
            return query, grad
        q = query.reshape(self.tokens, self.n, self.qw)
        g = grad.reshape(self.tokens, self.n, self.own)
        gap = self.wide - self.qw - self.own
        parts = [q] + ([jnp.zeros((*q.shape[:2], gap), bf16)] if gap else []) + [g]
        return jnp.concatenate(parts, axis=-1).transpose(1, 0, 2), grad


def fused_kernel(
    pn,
    query, grad, latent, rope_key, gain, kw, vw, move, rmove, cos_t, sin_t,
    dq_in, wg_out, latent_out, rope_out, gain_out,
    arrived, nlat_all, k_all, v_all, q_s, go_s, k_s, kt_s, v_s, s_s, dp_s, p_s, ds_s, dqt_s, tc_s, ts_s,
    latent_grad, rope_grad, gain_grad, dk_s, dv_s, dq_send, dk_send, dv_send, dr_s, dr_send, dr_in, dk_in, dv_in, part, pieces, summed, blocks, d_nlat, g_part, g_in, g_part2, g_in2,
    lsem, nsend, nrecv, wsend, wrecv, qsend, qrecv, rsend, rrecv, psend, precv, gsend, grecv, osend, orecv, asend, arecv, bsend, brecv,
):
    n, m, tokens, channels, tile = pn.n, pn.m, pn.tokens, pn.channels, pn.tile
    length, pairs, ratio, own = pn.length, pn.pairs, pn.ratio, pn.own
    s = lax.axis_index("sp")
    d = lax.axis_index("dp")
    ny = inner(n)
    nz = n // ny
    z, y = lax.div(s, ny), lax.rem(s, ny)
    x, c = lax.div(d, 2), lax.rem(d, 2)
    scale = WIDTH ** (-0.5)

    scopes = []

    def mark(name):
        if scopes:
            scopes.pop().__exit__(None, None, None)
        if name:
            scopes.append(jax.named_scope(name))
            scopes[-1].__enter__()

    def block(t):
        return pl.ds(pl.multiple_of(t * tokens, tokens), tokens)

    def at(b):
        return slice(b * tile, (b + 1) * tile)

    def source(move, t):
        which, lo, width, _ = move
        if which == 2:
            return query.at[t]
        ref, each = (query, pn.qw) if which == 0 else (grad, own)
        return ref.at[:, pl.ds(pl.multiple_of(t * each + lo, LANES), width)]

    def landing(move, t):
        return arrived.at[block(t), move[3] : move[3] + move[2]]

    spread = [(i, move) for i, moves in enumerate(pn.moves) for move in moves]

    def local_copies():
        made = [pltpu.make_async_copy(kw, k_all.at[d], lsem.at[0]), pltpu.make_async_copy(vw, v_all.at[d], lsem.at[1])]
        return made + [pltpu.make_async_copy(source(move, s), landing(move, s), lsem.at[3 + j]) for j, (_, move) in enumerate(spread)]

    for copy in local_copies():
        copy.start()
    mark("greet")
    bar = pltpu.get_barrier_semaphore()
    for k in range(1, n):
        pl.semaphore_signal(bar, inc=1, device_id=(lax.rem(s + k, n), d), device_id_type=MESH)
    for k in range(1, m):
        pl.semaphore_signal(bar, inc=1, device_id=(s, lax.rem(d + k, m)), device_id_type=MESH)

    lat = latent[...].astype(f32)
    inv_rms = lax.rsqrt(jnp.mean(lat * lat, axis=-1, keepdims=True) + eps)
    nlat_all[block(s), :channels] = (lat * inv_rms * gain[...]).astype(bf16)
    for b in range(pn.blocks):
        none = jnp.zeros((ROPE, tile), f32)
        co, si = cos_t[:, at(b)], sin_t[:, at(b)]
        tc_s[at(b), :] = jnp.concatenate([co, co, none, co, co, none], axis=0).T
        ts_s[at(b), :] = jnp.concatenate([-si, si, none, -si, si, none], axis=0).T
    turned = mm(rope_key[...], rmove[...], (((0,), (0,)), ((), ())))
    nlat_all[block(s), channels:] = (turned[:, :LANES] * tc_s[block(s), :] + turned[:, LANES:] * ts_s[block(s), :]).astype(bf16)
    dr_s[...] = jnp.zeros_like(dr_s)
    mark("bar_wait")
    pl.semaphore_wait(bar, n + m - 2)

    def member(a, b):
        return (a * ny + b, d)

    gs = []
    cut = tokens // PARTS
    for j in range(PARTS):
        def rows_of(t, j=j):
            return nlat_all.at[pl.ds(pl.multiple_of(t * tokens + j * cut, cut), cut)]
        gs.append(Gather(rows_of(s), rows_of, nz, ny, z, y, member, nsend.at[j], nrecv.at[j]))
    ws = []
    for j in range(ratio):
        rows = pl.ds(pl.multiple_of(lax.rem(s + j, ratio) * own, own), own)
        for i, (mine, whole) in enumerate(((kw, k_all), (vw, v_all))):
            ws.append(Gather(mine.at[rows], lambda t, whole=whole, rows=rows: whole.at[t, rows], m // 2, 2, x, c,
                             lambda a, b: (s, a * 2 + b), wsend.at[2 * j + i], wrecv.at[2 * j + i]))

    def others(act):
        lax.fori_loop(1, n, lambda k, _: (act(k, lax.rem(s + k, n)), 0)[1], 0)

    def moved(chunk, k, t):
        return [rcopy(source(move, t), landing(move, s), qsend.at[j, k], qrecv.at[j, k], (t, d)) for j, (i, move) in enumerate(spread) if i == chunk]

    def start_moved(chunk, when=None):
        def act(k, t):
            def go():
                for copy in moved(chunk, k, t):
                    copy.start()
            if when is None:
                go()
            else:
                pl.when(when(lax.div(t, ny)))(go)
        others(act)

    mark("gather")
    for g in gs:
        g.begin()
    for w in ws:
        w.begin()
    for i in range(nz):
        if i:
            for g in gs:
                g.line(i)

        @pl.when(z == i)
        def _():
            start_moved(0, lambda tz: tz > z)

        @pl.when(nz - 1 - z == i)
        def _():
            start_moved(0, lambda tz: tz < z)

    start_moved(0, lambda tz: tz == z)
    for chunk in range(1, len(pn.chunks)):
        start_moved(chunk)
    mark("w_line")
    for w in ws[:2]:
        for k in range(1, m // 2):
            w.line(k)
    mark("across")
    for j in range(1, ny):
        for g in gs:
            g.across(j)
    for w in ws[:2]:
        w.across(1)
    for copy in local_copies():
        copy.wait()
    for w in ws[2:]:
        for k in range(1, m // 2):
            w.line(k)

    mark("project")
    holder = lax.div(s, ratio)
    mine = pl.ds(pl.multiple_of(lax.rem(s, ratio) * own, own), own)

    def project(b, _):
        rows = pl.ds(pl.multiple_of(b * tile, tile), tile)
        a = nlat_all[rows, :channels]
        keys = mm(a, k_all[holder, mine, :], NT).astype(bf16)
        vals = mm(a, v_all[holder, mine, :], NT).astype(bf16)
        for p in range(pairs):
            dk_send[p, rows, :] = keys[:, p * LANES : (p + 1) * LANES]
            dv_send[p, rows, :] = vals[:, p * LANES : (p + 1) * LANES]
        return 0

    lax.fori_loop(0, pn.blocks, project, 0)

    lane = lax.broadcasted_iota(jnp.int32, (tile, LANES), 1)
    low = lane < PLAIN

    def returned(p, i, k, t):
        lo, hi = pn.dq_cols[p]
        cols = pl.ds(pl.multiple_of(s * own + p * LANES, LANES), LANES)
        if i == 0:
            src, dst = dk_send.at[p, block(t)], dk_in.at[:, cols]
        elif i == 1:
            src, dst = dv_send.at[p, block(t)], dv_in.at[:, cols]
        else:
            src = dq_send.at[block(t), lo:hi]
            dst = dq_in.at[:, pl.ds(pl.multiple_of(s * pn.qw + lo, LANES), hi - lo)] if pn.aligned else dq_in.at[s]
        return rcopy(src, dst, rsend.at[3 * p + i, k], rrecv.at[3 * p + i, k], (t, d))

    def has_dq(p):
        return pn.dq_cols[p][1] > pn.dq_cols[p][0]

    def own_copies(p):
        cols = pl.ds(pl.multiple_of(s * own + p * LANES, LANES), LANES)
        dk_in[:, cols] = dk_send[p, block(s), :]
        dv_in[:, cols] = dv_send[p, block(s), :]

    def dq_own():
        if pn.aligned:
            return pltpu.make_async_copy(dq_send.at[block(s)], dq_in.at[:, pl.ds(pl.multiple_of(s * pn.qw, LANES), pn.qw)], lsem.at[2])
        return pltpu.make_async_copy(dq_send.at[block(s)], dq_in.at[s], lsem.at[2])

    def pieces_of(p):
        return [t for t in range(m) if t * pn.rows // LANES % pairs == p]

    def part_copy(t, j):
        return rcopy(part.at[t], pieces.at[j], psend.at[t], precv.at[j], (s, t))

    def weight_parts(p):
        for i, src in ((p, dk_send), (pairs + p, dv_send)):
            out = mm(src[p], nlat_all[:, :channels], (((0,), (0,)), ((), ()))).astype(bf16)
            for r in range(0, LANES, pn.rows):
                part[(i * LANES + r) // pn.rows] = out[r : r + pn.rows]
        for t in pieces_of(p):
            @pl.when(t != d)
            def _():
                part_copy(t, d).start()

    def pair(p, _):
        for q in range(pairs):
            @pl.when(p == q)
            def _():
                if q < len(pn.chunks):
                    with jax.named_scope(f"chunk_wait{q}"):
                        others(lambda k, t: [copy.wait_recv() for copy in moved(q, k, t)])
                t0, t1 = pn.q_tiles[q]

                def prepare(b, _):
                    rows = pl.ds(pl.multiple_of(b * tile, tile), tile)
                    xs = jnp.concatenate([arrived[rows, t0 * LANES : (t0 + 1) * LANES], arrived[rows, t1 * LANES : (t1 + 1) * LANES]], axis=1)
                    out = mm(xs, move[q % 2])
                    tc, ts = tc_s[rows, :], ts_s[rows, :]
                    q_s[0, rows, :] = (out[:, :LANES] * jnp.where(low, 1.0, tc) + out[:, LANES : 2 * LANES] * ts).astype(bf16)
                    q_s[1, rows, :] = (out[:, 2 * LANES : 3 * LANES] * jnp.where(low, tc, 1.0) + out[:, 3 * LANES :] * ts).astype(bf16)
                    go_s[rows, :] = arrived[rows, pn.go_tile[q] * LANES : (pn.go_tile[q] + 1) * LANES]
                    return 0

                lax.fori_loop(0, pn.blocks, prepare, 0)

        for b in range(pn.blocks):
            kp, vp, rp = dk_send[p, at(b), :], dv_send[p, at(b), :], nlat_all[at(b), channels:]
            none = jnp.zeros_like(vp)
            even, odd = jnp.where(low, kp, rp), jnp.where(low, rp, kp)
            k_s[0, at(b), :] = even
            k_s[1, at(b), :] = odd
            kt_s[0, :, at(b)] = even.astype(f32).T.astype(bf16)
            kt_s[1, :, at(b)] = odd.astype(f32).T.astype(bf16)
            v_s[0, at(b), :] = jnp.where(low, vp, none)
            v_s[1, at(b), :] = jnp.where(low, none, vp)

        def put_dq(h):
            def put(cols, plain, back):
                dqt_s[p, h * WIDTH : h * WIDTH + PLAIN, cols] = plain
                dqt_s[p, h * WIDTH + PLAIN : (h + 1) * WIDTH, cols] = back
            return put

        def put_kv(h):
            def put(rows, dk, dv):
                if h == 0:
                    dk_send[p, rows, :] = dk.astype(bf16)
                    dv_send[p, rows, :] = dv.astype(bf16)
                    dr_s[rows, :] += jnp.where(low, 0.0, dk)
                else:
                    dk_send[p, rows, :] = jnp.where(low, dk_send[p, rows, :], dk.astype(bf16))
                    dv_send[p, rows, :] = jnp.where(low, dv_send[p, rows, :], dv.astype(bf16))
                    dr_s[rows, :] += jnp.where(low, dk, 0.0)
            return put

        with jax.named_scope("core"):
          pair_backward(tile, [(h == 1, q_s.at[h], go_s, k_s.at[h], kt_s.at[h], v_s.at[h], put_dq(h), put_kv(h)) for h in range(2)],
                      cos_t, sin_t, s_s, dp_s, p_s, ds_s, *(() if pn.hold else (dk_s, dv_s)))

        for q in range(pairs):
            @pl.when(p == q)
            def _():
                lo, hi = pn.dq_cols[q]
                for b in range(pn.blocks):
                    if hi > lo:
                        rows = [dqt_s[i // (2 * WIDTH), i % (2 * WIDTH) : i % (2 * WIDTH) + 64, at(b)] for i in range(lo, hi, 64)]
                        dq_send[at(b), lo:hi] = jnp.concatenate(rows, axis=0).astype(f32).T.astype(bf16)
                if q < pairs - 1:
                    for i in range(3 if has_dq(q) else 2):
                        others(lambda k, t: returned(q, i, k, t).start())
                own_copies(q)
                weight_parts(q)
        return 0

    mark("pairs")
    lax.fori_loop(0, pairs, pair, 0)

    mark("dr")
    quarter = tokens // 4
    both = dr_s[:, :ROPE] + dr_s[:, PLAIN : PLAIN + ROPE]
    for t in range(n):
        dr_send[t] = jnp.concatenate([both[t * tokens + j * quarter : t * tokens + (j + 1) * quarter] for j in range(4)], axis=1)
    dr_in[s] = dr_send[s]

    def dr_copy(k, t):
        return rcopy(dr_send.at[t], dr_in.at[s], asend.at[1, k], arecv.at[1, k], (t, d))


    mark("part_wait")
    pieces[d] = part[d]
    for j in range(m):
        @pl.when(j != d)
        def _():
            part_copy(0, j).wait_recv()
    total = pieces[0].astype(f32)
    for j in range(1, m):
        total = total + pieces[j].astype(f32)
    summed[...] = total.astype(bf16)

    wg = Gather(summed, lambda t: blocks.at[t], nz, ny, z, y, member, gsend, grecv)

    def place_of(slot, j):
        rows = pl.ds(pl.multiple_of(lax.rem(slot, ratio) * own + lax.rem(j, m // 2) * pn.rows, pn.rows), pn.rows)
        return wg_out.at[lax.div(j, m // 2), rows]

    def pass_on(slot, src):
        owner, place = lax.div(slot, ratio), lax.rem(slot, ratio)

        @pl.when(owner != d)
        def _():
            rcopy(src, place_of(slot, d), osend.at[slot], orecv.at[place, d], (s, owner)).start()

        @pl.when(owner == d)
        def _():
            pltpu.make_async_copy(src, place_of(slot, d), osend.at[slot]).start()

    mark("wg_line")
    wg.begin()
    pass_on(s, summed)
    dq_own().start()
    final = pairs - 1
    others(lambda k, t: returned(final, 0, k, t).start())
    for i in range(1, nz):
        wg.line(i, lambda slot: pass_on(slot, blocks.at[slot]))
        if i == 1:
            others(lambda k, t: returned(final, 1, k, t).start())
        if i == min(2, nz - 1):
            others(lambda k, t: dr_copy(k, t).start())
            others(lambda k, t: returned(final, 2, k, t).start())
    mark("wg_across")
    for j in range(1, ny):
        wg.across(j, lambda slot: pass_on(slot, blocks.at[slot]))
    mark("kv_wait")
    for p in range(pairs):
        for i in range(2):
            others(lambda k, t: returned(p, i, k, t).wait_recv())
    mark("w_rest")
    for w in ws[2:]:
        w.across(1)
    mark("d_nlat")
    for t in range(m):
        cols = slice(t * ratio * own, (t + 1) * ratio * own)
        term = mm(dk_in[:, cols], k_all[t]) + mm(dv_in[:, cols], v_all[t])
        if t == 0:
            d_nlat[...] = term
        else:
            d_nlat[...] += term
    lat = latent[...].astype(f32)
    inv_rms = lax.rsqrt(jnp.mean(lat * lat, axis=-1, keepdims=True) + eps)
    normed = lat * inv_rms
    dn = d_nlat[...]
    sums = jnp.sum(dn * normed, axis=0, keepdims=True)
    g_part[...] = jnp.concatenate([sums[:, i * LANES : (i + 1) * LANES] for i in range(channels // LANES)], axis=0)

    def first_round(k, t):
        return rcopy(g_part, g_in.at[k], asend.at[0, k], arecv.at[0, k], (t, d))

    others(lambda k, t: first_round(k, t).start())
    scaled = dn * gain[...]
    latent_grad[...] = inv_rms * (scaled - normed * jnp.mean(scaled * normed, axis=-1, keepdims=True))
    results = [pltpu.make_async_copy(latent_grad, latent_out, lsem.at[7])]
    results[0].start()

    mark("gain1")
    others(lambda k, t: first_round(k, t).wait_recv())
    g_in[0] = g_part[...]
    total = g_in[lax.rem(s + n, n)]
    for t in range(1, n):
        total = total + g_in[lax.rem(s - t + n, n)]
    g_part2[...] = total
    second_round = [rcopy(g_part2, g_in2.at[k], bsend.at[k], brecv.at[k], (s, lax.rem(d + k, m))) for k in range(1, m)]
    for copy in second_round:
        copy.start()

    mark("dr_sum")
    others(lambda k, t: dr_copy(k, t).wait_recv())
    total = dr_in[0]
    for t in range(1, n):
        total = total + dr_in[t]
    summed_dr = jnp.concatenate([total[:, j * ROPE : (j + 1) * ROPE] for j in range(4)], axis=0)
    half = ROPE // 2
    co, si = tc_s[block(s), :half], ts_s[block(s), half:ROPE]
    a, b = summed_dr[:, :half], summed_dr[:, half:]
    rope_grad[...] = jnp.concatenate([a * co + b * si, b * co - a * si], axis=1).T
    results.append(pltpu.make_async_copy(rope_grad, rope_out, lsem.at[8]))
    results[1].start()

    mark("dq_wait")
    for p in range(pairs):
        if has_dq(p):
            others(lambda k, t: returned(p, 2, k, t).wait_recv())
    mark("wgo_wait")
    for p in range(m):
        @pl.when(p != d)
        def _():
            for place in range(ratio):
                rcopy(summed, place_of(place, p), osend.at[0], orecv.at[place, p], (s, p)).wait_recv()
    for copy in second_round:
        copy.wait_recv()
    g_in2[0] = g_part2[...]
    total = g_in2[lax.rem(d + m, m)]
    for t in range(1, m):
        total = total + g_in2[lax.rem(d - t + m, m)]
    for i in range(channels // LANES):
        gain_grad[:, i * LANES : (i + 1) * LANES] = total[i : i + 1, :]
    results.append(pltpu.make_async_copy(gain_grad, gain_out, lsem.at[9]))
    results[2].start()

    mark("drain")
    for g in gs:
        g.finish()
    for w in ws:
        w.finish()
    wg.finish()
    def sent(k, t):
        for chunk in range(len(pn.chunks)):
            for copy in moved(chunk, k, t):
                copy.wait_send()
        for p in range(pairs):
            for i in range(3 if has_dq(p) else 2):
                returned(p, i, k, t).wait_send()
        dr_copy(k, t).wait_send()
        first_round(k, t).wait_send()

    others(sent)
    for t in range(m):
        @pl.when(t != d)
        def _():
            part_copy(t, d).wait_send()
    for copy in second_round:
        copy.wait_send()
    dq_own().wait()
    for copy in results:
        copy.wait()
    for slot in range(n):
        owner, place = slot // ratio, slot % ratio

        @pl.when(owner != d)
        def _():
            rcopy(summed, place_of(slot, d), osend.at[slot], orecv.at[place, d], (s, owner)).wait_send()

        @pl.when(owner == d)
        def _():
            pltpu.make_async_copy(summed, place_of(slot, d), osend.at[slot]).wait()
    mark(None)


def fused(pn, query, grad, latent, rope_key, gain, kw, vw):
    n, m, tokens, channels, length, pairs, tile = pn.n, pn.m, pn.tokens, pn.channels, pn.length, pn.pairs, pn.tile
    cos_t, sin_t = tables(length)
    A = pl.BlockSpec(memory_space=pl.ANY)
    V = pl.BlockSpec(memory_space=pltpu.VMEM)
    S = pltpu.SemaphoreType.DMA
    M = pltpu.VMEM
    piece = (pn.rows, channels)
    held = (pn.depth, (pn.blocks + 1) // 2, tile, (pn.blocks + 1) * tile) if pn.hold else (1, pn.blocks, tile, tile)
    acc = (8, LANES) if pn.hold else (length, LANES)
    outs = (
        jax.ShapeDtypeStruct((tokens, n * pn.qw) if pn.aligned else (n, tokens, pn.qw), bf16),
        jax.ShapeDtypeStruct((2, pn.ratio * pn.own, channels), bf16),
        jax.ShapeDtypeStruct((tokens, channels), f32),
        jax.ShapeDtypeStruct((ROPE, tokens), f32),
        jax.ShapeDtypeStruct((1, channels), f32),
    )
    scratch = [
        M((length, pn.wide), bf16), M((length, channels + LANES), bf16), M((m, *kw.shape), bf16), M((m, *vw.shape), bf16),
        M((2, length, LANES), bf16), M((length, LANES), bf16), M((2, length, LANES), bf16), M((2, LANES, length), bf16), M((2, length, LANES), bf16),
        M((pn.depth, length, tile), f32), M((pn.depth, length, tile), f32), M(held, bf16), M(held, bf16),
        M((pairs, 2 * WIDTH, length), bf16), M((length, LANES), f32), M((length, LANES), f32),
        M((tokens, channels), f32), M((ROPE, tokens), f32), M((1, channels), f32), M(acc, f32), M(acc, f32),
        M((length, pn.qw), bf16), M((pairs, length, LANES), bf16), M((pairs, length, LANES), bf16),
        M((length, LANES), f32), M((n, tokens // 4, LANES), f32), M((n, tokens // 4, LANES), f32),
        M((tokens, n * pn.own), bf16), M((tokens, n * pn.own), bf16),
        M((m, *piece), bf16), M((m, *piece), bf16), M(piece, bf16), M((n, *piece), bf16), M((tokens, channels), f32),
        M((channels // LANES, LANES), f32), M((n, channels // LANES, LANES), f32), M((channels // LANES, LANES), f32), M((m, channels // LANES, LANES), f32),
        S((10,)), S((PARTS, n, 4)), S((PARTS, n)), S((2 * pn.ratio, m, 4)), S((2 * pn.ratio, m)), S((4, n)), S((4, n)), S((3 * pairs, n)), S((3 * pairs, n)),
        S((m,)), S((m,)), S((n, 4)), S((n,)), S((n,)), S((pn.ratio, m)), S((2, n)), S((2, n)), S((m,)), S((m,)),
    ]
    return pl.pallas_call(
        functools.partial(fused_kernel, pn), out_shape=outs,
        in_specs=[A, A, V, V, V, A, A, V, V, V, V], out_specs=(A,) * 5, scratch_shapes=scratch,
        compiler_params=pltpu.CompilerParams(collective_id=11, has_side_effects=True, vmem_limit_bytes=64 * 1024 * 1024 - 64 * 1024),
    )(query, grad, latent, rope_key, gain, kw, vw, jnp.asarray(head_mover(pairs), bf16), jnp.asarray(rope_mover(), bf16), jnp.asarray(cos_t), jnp.asarray(sin_t))


def local(query, latent, rope_key, gain, key_up, value_up, out_grad):
    sp = lax.axis_size("sp")
    dp = lax.axis_size("dp")
    tokens, channels = latent.shape[1:]
    pn = Plan(sp, dp, tokens, channels)
    query, out_grad = pn.pack(query[0], out_grad[0])
    dq, wg, latent_grad, rope_grad, gain_grad = fused(pn, query, out_grad, latent[0], rope_key[0].T, gain[None], key_up, value_up)
    query_grad = dq if pn.aligned else dq.transpose(1, 0, 2).reshape(tokens, -1)
    return (query_grad[None], latent_grad[None], rope_grad.T[None], wg[0].astype(f32), wg[1].astype(f32), gain_grad[0])


def solution(mesh):
    tok = P("dp", "sp", None)
    rows = P("dp", None)
    return jax.shard_map(local, mesh=mesh, in_specs=(tok, tok, tok, P(), rows, rows, tok), out_specs=(tok, tok, tok, rows, rows, P()), check_vma=False)
```

time: 331 us -> 180 us (0.54)
  Pallas kernels: 244 us -> 171 us
  blocking collectives: 37.7 us -> 0 us
  other arithmetic: 19.1 us -> 4.11 us
  matrix products: 13.9 us -> 0 us
  local copies, waits for them, and re-layouts: 12.9 us -> 3.65 us
    pallas_call x3 -> x1, Pallas kernels: 244 us -> 171 us  [fused(): pl.pallas_call(functools.partial(fused_kernel, pn), out_shape=outs, in_sp...]
    psum x1 -> x0, blocking collectives: 37.7 us -> none  [local(): gain_grad = lax.psum(jnp.sum(d_nlat * normed, axis=0), ('sp', 'dp'))]
    dot_general x6 -> x0, matrix products: 13.9 us -> none  [the longest x1 3.39 us: local(): d_nlat = d_nlat + lax.dot_general(dv, v_all, NN, preferred_element_type=f32)]
    another operation x4 -> x0, other arithmetic: 4.65 us -> none  [the longest x2 2.26 us: local(): jnp.stack([jnp.concatenate([arrived[:, p * 2 * WIDTH:(p + 1) * 2 * WIDTH]...]
    slice x4 -> x0, local copies, waits for them, and re-layouts: 4.54 us -> none  [the longest x1 2.32 us: local(): wg[:, 1].reshape(-1, channels)]
where the time goes in v2:
time: 180 us; the launch traced here: 179 us
  Pallas kernels  171 us (95%)
  other arithmetic  4.11 us (2%)
  local copies, waits for them, and re-layouts  3.65 us (2%)
    pallas_call x1, Pallas kernels, fused(): pl.pallas_call(functools.partial(fused_kernel, pn), out_shape=outs, in_sp...  171 us
    convert_element_type x1, other arithmetic, local(): wg[1].astype(f32)  4.11 us
    unnamed x12, local copies, waits for them, and re-layouts  3.65 us

profile of v2, /device:TPU:3, one launch (start us, length us, event | category | flops | bytes accessed | tf_op | source)
XLA Modules:
  0.0 179.4 jit_solution(11817873707144452069)
XLA Ops:
  0.6 170.9 %shard_map.154 = (bf16[192,3072]{1,0:T(8,128)(2,1)}, bf16[2,512,1024]{2,1,0:T(8,128)(2,1)}, f32[192,1024]{1,0:T(8,128)}, f32[32,192]{1,0:T(8,128)}, f32[1,1024]{1,0:T(1,128)}) custom-call(bf16[192,3072]{1,0:T(8,128)(2,1)} %bitcast.20, bf16[192,2048]{1,0:T(8,128)(2,1)} %bitcast.22, bf16[192,1024]{1,0:T(8,128)(2,1)} %bitcast.23, bf16[32,192]{1,0:T(8,128)(2,1)} %bitcast.25, ...), custom_call_target="tpu_custom_call" | custom-call | tf_op jit(solution)/shard_map/pallas_call | solution.py:757
  171.6 0.0 copy-start
  171.6 4.1 %bitcast_convert_fusion = (f32[512,1024]{1,0:T(8,128)}, f32[512,1024]{1,0:T(8,128)}) fusion(bf16[2,512,1024]{2,1,0:T(8,128)(2,1)} %get-tuple-element.14), kind=kLoop, calls=%fused_computation | loop fusion | flops 1048576 | bytes 6291456 | tf_op jit(solution)/shard_map/convert_element_type | solution.py:772
  175.7 0.0 copy-start.1
  175.7 0.0 copy-start.2
  175.7 0.0 copy-start.3
  175.7 0.0 copy-done
  175.7 1.0 copy.21
  176.7 0.5 copy-done.1
  177.3 0.9 copy.22
  178.1 0.0 copy-done.2
  178.1 0.6 copy.23
  178.8 0.0 copy-done.3
  178.8 0.6 copy.24
Async XLA Ops:
  171.6 4.1 %copy-start = (bf16[192,3072]{1,0:T(8,128)(2,1)S(1)}, bf16[192,3072]{1,0:T(8,128)(2,1)}, u32[]{:S(2)}) copy-start(bf16[192,3072]{1,0:T(8,128)(2,1)} %get-tuple-element.11) | copy-start | bytes 3538948
  175.7 1.6 copy-start.1
  175.7 2.4 %copy-start.2 = (f32[32,192]{1,0:T(8,128)S(1)}, f32[32,192]{1,0:T(8,128)}, u32[]{:S(2)}) copy-start(f32[32,192]{1,0:T(8,128)} %get-tuple-element.13) | copy-start | bytes 73732
  175.7 3.1 %copy-start.3 = (f32[1,1024]{1,0:T(1,128)S(1)}, f32[1,1024]{1,0:T(1,128)}, u32[]{:S(2)}) copy-start(f32[1,1024]{1,0:T(1,128)} %get-tuple-element.15) | copy-start | bytes 12292

commit v3 on v2

--- a/solution.py
+++ b/solution.py
@@ -226,6 +226,14 @@
     return m
 
 
+def rope_unfold():
+    m = np.zeros((4, LANES, LANES), np.float32)
+    for j in range(4):
+        for i in range(ROPE):
+            m[j, j * ROPE + i, i] = m[j, j * ROPE + i, PLAIN + i] = 1
+    return m
+
+
 def rope_mover():
     m = np.zeros((ROPE, 2 * LANES), np.float32)
     for i in range(ROPE):
@@ -281,9 +289,9 @@
 
 def fused_kernel(
     pn,
-    query, grad, latent, rope_key, gain, kw, vw, move, rmove, cos_t, sin_t,
+    query, grad, latent, rope_key, gain, kw, vw, move, rmove, unfold, cos_t, sin_t,
     dq_in, wg_out, latent_out, rope_out, gain_out,
-    arrived, nlat_all, k_all, v_all, q_s, go_s, k_s, kt_s, v_s, s_s, dp_s, p_s, ds_s, dqt_s, tc_s, ts_s,
+    arrived, nlat_all, rope_all, rope2, k_all, v_all, q_s, go_s, k_s, kt_s, v_s, s_s, dp_s, p_s, ds_s, dqt_s, tc_s, ts_s,
     latent_grad, rope_grad, gain_grad, dk_s, dv_s, dq_send, dk_send, dv_send, dr_s, dr_send, dr_in, dk_in, dv_in, part, pieces, summed, blocks, d_nlat, g_part, g_in, g_part2, g_in2,
     lsem, nsend, nrecv, wsend, wrecv, qsend, qrecv, rsend, rrecv, psend, precv, gsend, grecv, osend, orecv, asend, arecv, bsend, brecv,
 ):
@@ -339,14 +347,20 @@
 
     lat = latent[...].astype(f32)
     inv_rms = lax.rsqrt(jnp.mean(lat * lat, axis=-1, keepdims=True) + eps)
-    nlat_all[block(s), :channels] = (lat * inv_rms * gain[...]).astype(bf16)
+    nlat_all[block(s), :] = (lat * inv_rms * gain[...]).astype(bf16)
     for b in range(pn.blocks):
         none = jnp.zeros((ROPE, tile), f32)
         co, si = cos_t[:, at(b)], sin_t[:, at(b)]
         tc_s[at(b), :] = jnp.concatenate([co, co, none, co, co, none], axis=0).T
         ts_s[at(b), :] = jnp.concatenate([-si, si, none, -si, si, none], axis=0).T
     turned = mm(rope_key[...], rmove[...], (((0,), (0,)), ((), ())))
-    nlat_all[block(s), channels:] = (turned[:, :LANES] * tc_s[block(s), :] + turned[:, LANES:] * ts_s[block(s), :]).astype(bf16)
+    turned = turned[:, :LANES] * tc_s[block(s), :] + turned[:, LANES:] * ts_s[block(s), :]
+    quarter = tokens // 4
+
+    def four(t):
+        return pl.ds(pl.multiple_of(t * quarter, quarter), quarter)
+
+    rope_all[four(s), :] = jnp.concatenate([turned[j * quarter : (j + 1) * quarter, :ROPE] for j in range(4)], axis=1).astype(bf16)
     dr_s[...] = jnp.zeros_like(dr_s)
     mark("bar_wait")
     pl.semaphore_wait(bar, n + m - 2)
@@ -360,6 +374,7 @@
         def rows_of(t, j=j):
             return nlat_all.at[pl.ds(pl.multiple_of(t * tokens + j * cut, cut), cut)]
         gs.append(Gather(rows_of(s), rows_of, nz, ny, z, y, member, nsend.at[j], nrecv.at[j]))
+    gs.append(Gather(rope_all.at[four(s)], lambda t: rope_all.at[four(t)], nz, ny, z, y, member, nsend.at[PARTS], nrecv.at[PARTS]))
     ws = []
     for j in range(ratio):
         rows = pl.ds(pl.multiple_of(lax.rem(s + j, ratio) * own, own), own)
@@ -405,37 +420,48 @@
     start_moved(0, lambda tz: tz == z)
     for chunk in range(1, len(pn.chunks)):
         start_moved(chunk)
-    mark("w_line")
-    for w in ws[:2]:
-        for k in range(1, m // 2):
-            w.line(k)
-    mark("across")
-    for j in range(1, ny):
-        for g in gs:
-            g.across(j)
-    for w in ws[:2]:
-        w.across(1)
-    for copy in local_copies():
-        copy.wait()
-    for w in ws[2:]:
-        for k in range(1, m // 2):
-            w.line(k)
-
-    mark("project")
     holder = lax.div(s, ratio)
     mine = pl.ds(pl.multiple_of(lax.rem(s, ratio) * own, own), own)
 
-    def project(b, _):
-        rows = pl.ds(pl.multiple_of(b * tile, tile), tile)
-        a = nlat_all[rows, :channels]
+    def project(t):
+        rows = block(t)
+        a = nlat_all[rows, :]
         keys = mm(a, k_all[holder, mine, :], NT).astype(bf16)
         vals = mm(a, v_all[holder, mine, :], NT).astype(bf16)
         for p in range(pairs):
             dk_send[p, rows, :] = keys[:, p * LANES : (p + 1) * LANES]
             dv_send[p, rows, :] = vals[:, p * LANES : (p + 1) * LANES]
+
+    mark("w_line")
+    for w in ws[:2]:
+        for k in range(1, m // 2):
+            w.line(k)
+    for w in ws[:2]:
+        w.across(1)
+    for copy in local_copies():
+        copy.wait()
+    mark("project1")
+    lax.fori_loop(0, nz, lambda a, _: (project(a * ny + y), 0)[1], 0)
+    mark("across")
+    for j in range(1, ny):
+        for g in gs:
+            g.across(j)
+    for w in ws[2:]:
+        for k in range(1, m // 2):
+            w.line(k)
+    mark("project2")
+
+    def rest(t, _):
+        @pl.when(lax.rem(t, ny) != y)
+        def _():
+            project(t)
         return 0
 
-    lax.fori_loop(0, pn.blocks, project, 0)
+    lax.fori_loop(0, n, rest, 0)
+    for j in range(4):
+        out = mm(rope_all[...], unfold[j]).astype(bf16)
+        for t in range(n):
+            rope2[t * tokens + j * quarter : t * tokens + (j + 1) * quarter, :] = out[t * quarter : (t + 1) * quarter]
 
     lane = lax.broadcasted_iota(jnp.int32, (tile, LANES), 1)
     low = lane < PLAIN
@@ -473,7 +499,7 @@
 
     def weight_parts(p):
         for i, src in ((p, dk_send), (pairs + p, dv_send)):
-            out = mm(src[p], nlat_all[:, :channels], (((0,), (0,)), ((), ()))).astype(bf16)
+            out = mm(src[p], nlat_all[...], (((0,), (0,)), ((), ()))).astype(bf16)
             for r in range(0, LANES, pn.rows):
                 part[(i * LANES + r) // pn.rows] = out[r : r + pn.rows]
         for t in pieces_of(p):
@@ -503,7 +529,7 @@
                 lax.fori_loop(0, pn.blocks, prepare, 0)
 
         for b in range(pn.blocks):
-            kp, vp, rp = dk_send[p, at(b), :], dv_send[p, at(b), :], nlat_all[at(b), channels:]
+            kp, vp, rp = dk_send[p, at(b), :], dv_send[p, at(b), :], rope2[at(b), :]
             none = jnp.zeros_like(vp)
             even, odd = jnp.where(low, kp, rp), jnp.where(low, rp, kp)
             k_s[0, at(b), :] = even
@@ -554,16 +580,17 @@
     lax.fori_loop(0, pairs, pair, 0)
 
     mark("dr")
-    quarter = tokens // 4
     both = dr_s[:, :ROPE] + dr_s[:, PLAIN : PLAIN + ROPE]
     for t in range(n):
-        dr_send[t] = jnp.concatenate([both[t * tokens + j * quarter : t * tokens + (j + 1) * quarter] for j in range(4)], axis=1)
+        dr_send[t] = jnp.concatenate([both[t * tokens + j * quarter : t * tokens + (j + 1) * quarter] for j in range(4)], axis=1).astype(bf16)
     dr_in[s] = dr_send[s]
 
     def dr_copy(k, t):
         return rcopy(dr_send.at[t], dr_in.at[s], asend.at[1, k], arecv.at[1, k], (t, d))
 
 
+    final = pairs - 1
+    others(lambda k, t: returned(final, 0, k, t).start())
     mark("part_wait")
     pieces[d] = part[d]
     for j in range(m):
@@ -596,49 +623,68 @@
     wg.begin()
     pass_on(s, summed)
     dq_own().start()
-    final = pairs - 1
-    others(lambda k, t: returned(final, 0, k, t).start())
-    for i in range(1, nz):
-        wg.line(i, lambda slot: pass_on(slot, blocks.at[slot]))
+    others(lambda k, t: returned(final, 1, k, t).start())
+    results = []
+
+    def first_round(k, t):
+        return rcopy(g_part, g_in.at[k], asend.at[0, k], arecv.at[0, k], (t, d))
+
+    def turn_back():
+        mark("kv_wait")
+        for p in range(pairs):
+            for i in range(2):
+                others(lambda k, t: returned(p, i, k, t).wait_recv())
+        mark("w_rest")
+        for w in ws[2:]:
+            w.across(1)
+        mark("d_nlat")
+        for t in range(m):
+            cols = slice(t * ratio * own, (t + 1) * ratio * own)
+            term = mm(dk_in[:, cols], k_all[t]) + mm(dv_in[:, cols], v_all[t])
+            if t == 0:
+                d_nlat[...] = term
+            else:
+                d_nlat[...] += term
+        lat = latent[...].astype(f32)
+        inv_rms = lax.rsqrt(jnp.mean(lat * lat, axis=-1, keepdims=True) + eps)
+        normed = lat * inv_rms
+        dn = d_nlat[...]
+        sums = jnp.sum(dn * normed, axis=0, keepdims=True)
+        g_part[...] = jnp.concatenate([sums[:, i * LANES : (i + 1) * LANES] for i in range(channels // LANES)], axis=0)
+        others(lambda k, t: first_round(k, t).start())
+        scaled = dn * gain[...]
+        latent_grad[...] = inv_rms * (scaled - normed * jnp.mean(scaled * normed, axis=-1, keepdims=True))
+        results.append(pltpu.make_async_copy(latent_grad, latent_out, lsem.at[7]))
+        results[-1].start()
+
+    def send_dq(when):
+        def act(k, t):
+            @pl.when(when(lax.div(t, ny)))
+            def _():
+                returned(final, 2, k, t).start()
+        others(act)
+
+    for i in range(nz):
+        if i:
+            if i == nz - 1:
+                turn_back()
+                mark("wg_last")
+            wg.line(i, lambda slot: pass_on(slot, blocks.at[slot]))
         if i == 1:
-            others(lambda k, t: returned(final, 1, k, t).start())
-        if i == min(2, nz - 1):
             others(lambda k, t: dr_copy(k, t).start())
-            others(lambda k, t: returned(final, 2, k, t).start())
+
+        @pl.when(z == i)
+        def _():
+            send_dq(lambda tz: tz > z)
+
+        @pl.when(nz - 1 - z == i)
+        def _():
+            send_dq(lambda tz: tz < z)
+
+    send_dq(lambda tz: tz == z)
     mark("wg_across")
     for j in range(1, ny):
         wg.across(j, lambda slot: pass_on(slot, blocks.at[slot]))
-    mark("kv_wait")
-    for p in range(pairs):
-        for i in range(2):
-            others(lambda k, t: returned(p, i, k, t).wait_recv())
-    mark("w_rest")
-    for w in ws[2:]:
-        w.across(1)
-    mark("d_nlat")
-    for t in range(m):
-        cols = slice(t * ratio * own, (t + 1) * ratio * own)
-        term = mm(dk_in[:, cols], k_all[t]) + mm(dv_in[:, cols], v_all[t])
-        if t == 0:
-            d_nlat[...] = term
-        else:
-            d_nlat[...] += term
-    lat = latent[...].astype(f32)
-    inv_rms = lax.rsqrt(jnp.mean(lat * lat, axis=-1, keepdims=True) + eps)
-    normed = lat * inv_rms
-    dn = d_nlat[...]
-    sums = jnp.sum(dn * normed, axis=0, keepdims=True)
-    g_part[...] = jnp.concatenate([sums[:, i * LANES : (i + 1) * LANES] for i in range(channels // LANES)], axis=0)
-
-    def first_round(k, t):
-        return rcopy(g_part, g_in.at[k], asend.at[0, k], arecv.at[0, k], (t, d))
-
-    others(lambda k, t: first_round(k, t).start())
-    scaled = dn * gain[...]
-    latent_grad[...] = inv_rms * (scaled - normed * jnp.mean(scaled * normed, axis=-1, keepdims=True))
-    results = [pltpu.make_async_copy(latent_grad, latent_out, lsem.at[7])]
-    results[0].start()
-
     mark("gain1")
     others(lambda k, t: first_round(k, t).wait_recv())
     g_in[0] = g_part[...]
@@ -652,16 +698,16 @@
 
     mark("dr_sum")
     others(lambda k, t: dr_copy(k, t).wait_recv())
-    total = dr_in[0]
+    total = dr_in[0].astype(f32)
     for t in range(1, n):
-        total = total + dr_in[t]
+        total = total + dr_in[t].astype(f32)
     summed_dr = jnp.concatenate([total[:, j * ROPE : (j + 1) * ROPE] for j in range(4)], axis=0)
     half = ROPE // 2
     co, si = tc_s[block(s), :half], ts_s[block(s), half:ROPE]
     a, b = summed_dr[:, :half], summed_dr[:, half:]
     rope_grad[...] = jnp.concatenate([a * co + b * si, b * co - a * si], axis=1).T
     results.append(pltpu.make_async_copy(rope_grad, rope_out, lsem.at[8]))
-    results[1].start()
+    results[-1].start()
 
     mark("dq_wait")
     for p in range(pairs):
@@ -682,7 +728,7 @@
     for i in range(channels // LANES):
         gain_grad[:, i * LANES : (i + 1) * LANES] = total[i : i + 1, :]
     results.append(pltpu.make_async_copy(gain_grad, gain_out, lsem.at[9]))
-    results[2].start()
+    results[-1].start()
 
     mark("drain")
     for g in gs:
@@ -741,24 +787,59 @@
         jax.ShapeDtypeStruct((1, channels), f32),
     )
     scratch = [
-        M((length, pn.wide), bf16), M((length, channels + LANES), bf16), M((m, *kw.shape), bf16), M((m, *vw.shape), bf16),
+        M((length, pn.wide), bf16), M((length, channels), bf16), M((length // 4, LANES), bf16), M((length, LANES), bf16), M((m, *kw.shape), bf16), M((m, *vw.shape), bf16),
         M((2, length, LANES), bf16), M((length, LANES), bf16), M((2, length, LANES), bf16), M((2, LANES, length), bf16), M((2, length, LANES), bf16),
         M((pn.depth, length, tile), f32), M((pn.depth, length, tile), f32), M(held, bf16), M(held, bf16),
         M((pairs, 2 * WIDTH, length), bf16), M((length, LANES), f32), M((length, LANES), f32),
         M((tokens, channels), f32), M((ROPE, tokens), f32), M((1, channels), f32), M(acc, f32), M(acc, f32),
         M((length, pn.qw), bf16), M((pairs, length, LANES), bf16), M((pairs, length, LANES), bf16),
-        M((length, LANES), f32), M((n, tokens // 4, LANES), f32), M((n, tokens // 4, LANES), f32),
+        M((length, LANES), f32), M((n, tokens // 4, LANES), bf16), M((n, tokens // 4, LANES), bf16),
         M((tokens, n * pn.own), bf16), M((tokens, n * pn.own), bf16),
         M((m, *piece), bf16), M((m, *piece), bf16), M(piece, bf16), M((n, *piece), bf16), M((tokens, channels), f32),
         M((channels // LANES, LANES), f32), M((n, channels // LANES, LANES), f32), M((channels // LANES, LANES), f32), M((m, channels // LANES, LANES), f32),
-        S((10,)), S((PARTS, n, 4)), S((PARTS, n)), S((2 * pn.ratio, m, 4)), S((2 * pn.ratio, m)), S((4, n)), S((4, n)), S((3 * pairs, n)), S((3 * pairs, n)),
+        S((10,)), S((PARTS + 1, n, 4)), S((PARTS + 1, n)), S((2 * pn.ratio, m, 4)), S((2 * pn.ratio, m)), S((4, n)), S((4, n)), S((3 * pairs, n)), S((3 * pairs, n)),
         S((m,)), S((m,)), S((n, 4)), S((n,)), S((n,)), S((pn.ratio, m)), S((2, n)), S((2, n)), S((m,)), S((m,)),
     ]
     return pl.pallas_call(
         functools.partial(fused_kernel, pn), out_shape=outs,
-        in_specs=[A, A, V, V, V, A, A, V, V, V, V], out_specs=(A,) * 5, scratch_shapes=scratch,
+        in_specs=[A, A, V, V, V, A, A, V, V, V, V, V], out_specs=(A,) * 5, scratch_shapes=scratch,
         compiler_params=pltpu.CompilerParams(collective_id=11, has_side_effects=True, vmem_limit_bytes=64 * 1024 * 1024 - 64 * 1024),
-    )(query, grad, latent, rope_key, gain, kw, vw, jnp.asarray(head_mover(pairs), bf16), jnp.asarray(rope_mover(), bf16), jnp.asarray(cos_t), jnp.asarray(sin_t))
+    )(query, grad, latent, rope_key, gain, kw, vw, jnp.asarray(head_mover(pairs), bf16), jnp.asarray(rope_mover(), bf16), jnp.asarray(rope_unfold(), bf16), jnp.asarray(cos_t), jnp.asarray(sin_t))
+
+
+def finish_kernel(aligned, *refs):
+    if aligned:
+        refs[5][...] = refs[4][...]
+        refs = refs[:4] + refs[6:]
+    wg, latent, rope, gain, kw_out, vw_out, latent_out, rope_out, gain_out = refs
+    kw_out[...] = wg[0].astype(f32)
+    vw_out[...] = wg[1].astype(f32)
+    latent_out[...] = latent[...]
+    rope_out[...] = rope[...]
+    gain_out[...] = gain[...]
+
+
+def finish(dq, wg, latent, rope, gain, aligned):
+    steps = 4
+    weights = (wg.shape[1] // steps, wg.shape[2])
+
+    def rows(a):
+        return pl.BlockSpec((a.shape[0] // steps, a.shape[1]), lambda i: (i, 0))
+
+    def whole(a):
+        return pl.BlockSpec(a.shape, lambda i: (0, 0))
+
+    first = [dq] if aligned else []
+    ins = [wg, latent, rope, gain] + first
+    in_specs = [pl.BlockSpec((2, *weights), lambda i: (0, i, 0)), rows(latent), whole(rope), whole(gain)] + [rows(a) for a in first]
+    shape = jax.ShapeDtypeStruct(wg.shape[1:], f32)
+    outs = [jax.ShapeDtypeStruct(a.shape, a.dtype) for a in first] + [shape, shape] + [jax.ShapeDtypeStruct(a.shape, a.dtype) for a in (latent, rope, gain)]
+    out_specs = [rows(a) for a in first] + [rows(shape), rows(shape), rows(latent), whole(rope), whole(gain)]
+    done = pl.pallas_call(
+        functools.partial(finish_kernel, aligned), grid=(steps,), out_shape=outs, in_specs=in_specs, out_specs=out_specs,
+        compiler_params=pltpu.CompilerParams(dimension_semantics=("arbitrary",)),
+    )(*ins)
+    return done if aligned else [dq] + list(done)
 
 
 def local(query, latent, rope_key, gain, key_up, value_up, out_grad):
@@ -768,8 +849,9 @@
     pn = Plan(sp, dp, tokens, channels)
     query, out_grad = pn.pack(query[0], out_grad[0])
     dq, wg, latent_grad, rope_grad, gain_grad = fused(pn, query, out_grad, latent[0], rope_key[0].T, gain[None], key_up, value_up)
+    dq, kw, vw, latent_grad, rope_grad, gain_grad = finish(dq, wg, latent_grad, rope_grad, gain_grad, pn.aligned)
     query_grad = dq if pn.aligned else dq.transpose(1, 0, 2).reshape(tokens, -1)
-    return (query_grad[None], latent_grad[None], rope_grad.T[None], wg[0].astype(f32), wg[1].astype(f32), gain_grad[0])
+    return (query_grad[None], latent_grad[None], rope_grad.T[None], kw, vw, gain_grad[0])
 
 
 def solution(mesh):

time: 180 us -> 175 us (0.972)
  other arithmetic: 4.11 us -> 0 us
  local copies, waits for them, and re-layouts: 3.65 us -> 0 us
  Pallas kernels: 171 us -> 174 us
    pallas_call x0 -> x1, Pallas kernels: none -> 5.22 us  [finish(): pl.pallas_call(functools.partial(finish_kernel, aligned), grid=(steps,),...]
    convert_element_type x1 -> x0, other arithmetic: 4.11 us -> none  [local(): wg[1].astype(f32)]
    unnamed x12 -> x0, local copies, waits for them, and re-layouts: 3.65 us -> none
    pallas_call x1, Pallas kernels: 171 us -> 169 us  [fused(): pl.pallas_call(functools.partial(fused_kernel, pn), out_shape=outs, in_sp...]
where the time goes in v3:
time: 175 us
  Pallas kernels  174 us (99%)
    pallas_call x1, Pallas kernels, fused(): pl.pallas_call(functools.partial(fused_kernel, pn), out_shape=outs, in_sp...  169 us
    pallas_call x1, Pallas kernels, finish(): pl.pallas_call(functools.partial(finish_kernel, aligned), grid=(steps,),...  5.22 us

profile of v3, /device:TPU:3, one launch (start us, length us, event | category | flops | bytes accessed | tf_op | source)
XLA Modules:
  0.0 174.5 jit_solution(9090771404853355505)
XLA Ops:
  0.6 168.5 %shard_map.163 = (bf16[192,3072]{1,0:T(8,128)(2,1)}, bf16[2,512,1024]{2,1,0:T(8,128)(2,1)}, f32[192,1024]{1,0:T(8,128)}, f32[32,192]{1,0:T(8,128)}, f32[1,1024]{1,0:T(1,128)}) custom-call(bf16[192,3072]{1,0:T(8,128)(2,1)} %bitcast.13, bf16[192,2048]{1,0:T(8,128)(2,1)} %bitcast.14, bf16[192,1024]{1,0:T(8,128)(2,1)} %bitcast.15, bf16[32,192]{1,0:T(8,128)(2,1)} %bitcast.16, ...), custom_call_target="tpu_custom_call" | custom-call | tf_op jit(solution)/shard_map/pallas_call | solution.py:803
  169.2 5.2 %shard_map.164 = (bf16[192,3072]{1,0:T(8,128)(2,1)}, f32[512,1024]{1,0:T(8,128)}, f32[512,1024]{1,0:T(8,128)}, f32[192,1024]{1,0:T(8,128)}, f32[32,192]{1,0:T(8,128)}, /*index=5*/f32[1,1024]{1,0:T(1,128)}) custom-call(bf16[2,512,1024]{2,1,0:T(8,128)(2,1)} %get-tuple-element.17.refs_0_, f32[192,1024]{1,0:T(8,128)} %get-tuple-element.18.refs_1_, ...), custom_call_target="tpu_custom_call" | custom-call | tf_op jit(solution)/shard_map/pallas_call | solution.py:838
